TPU v7x, 32 devices: a whole 2x2x4 slice. The times are simulated.
32 devices in a mesh: sp: 8 (over z, y), tp: 4 (over x, core).
Axes of the slice: x: 2, y: 2, z: 4, core: 2. Of those that a mesh axis runs over, the one named last changes fastest.
Arguments:
- tokens: bfloat16 [3072, 4096], P(('sp', 'tp')), may hold values from -6 to 6
- norm_gain: float32 [4096], replicated, may hold values from 0.1 to 1.9
- w_query: bfloat16 [4096, 2048], P('sp', 'tp'), may hold values from -0.09375 to 0.09375
- w_key: bfloat16 [4096, 512], P('sp', 'tp'), may hold values from -1.5 to 1.5
- w_value: bfloat16 [4096, 512], P('sp', 'tp'), may hold values from -0.09375 to 0.09375
- w_mem_query: bfloat16 [4096, 1024], P('sp', 'tp'), may hold values from -0.09375 to 0.09375
- w_mem_key: bfloat16 [4096, 1024], P('sp', 'tp'), may hold values from -0.09375 to 0.09375
- w_mem_value: bfloat16 [4096, 1024], P('sp', 'tp'), may hold values from -0.09375 to 0.09375
- w_mem_gate: bfloat16 [4096, 1024], P('sp', 'tp'), may hold values from -0.09375 to 0.09375
- w_gates: bfloat16 [4096, 2, 16], replicated, may hold values from -0.09375 to 0.09375
- sinks: float32 [32], P('tp'), may hold values from 2 to 6
- forget_bias: float32 [16], P('tp'), may hold values from 3 to 13
- forget_shift: float32 [3072, 16], P('sp', 'tp'), may hold values from -1 to 0
- w_out: bfloat16 [3072, 4096], P('sp', 'tp'), may hold values from -0.21650635 to 0.21650635
Outputs:
- mixed: bfloat16 [3072, 4096], P('sp', 'tp')
- log_total: float32 [3072, 32], P('sp', 'tp')
All inputs are finite; a program needn't handle non-finite values.
Results may differ from a plain program's by a relative error of at most 0.018.
Values may be sent and summed in bfloat16 or wider, within the bound.
A program may use at most 128 MiB of HBM per device.

v0:
```python
import functools
import math

import jax
import jax.numpy as jnp
from jax import lax
from jax.experimental import pallas as pl
from jax.experimental.pallas import tpu as pltpu
from jax.sharding import PartitionSpec as P

HD = 64
WINDOW = 128
LANES = 128
EPSILON = 1e-06
MASKED = -1e30
MESH = pl.DeviceIdType.MESH


def begin(copy):
    copy.start()


def drain(copy):
    copy.wait_send()


def dot(left, right, **more):
    return jnp.dot(left, right, preferred_element_type=jnp.float32, **more)


def lanes_of(shape):
    return lax.broadcasted_iota(jnp.int32, shape, len(shape) - 1)


def mixer_kernel(
    sizes,
    tokens, gain, packed, shifts, gate_cols, w_out, sinks, bias,
    mixed, totals,
    T, W, GW, O, ACC, PROJ, NUM, ST, EB, HALO, FS, JS, J, LS, LT, LTF, X,
    own_sems, w_send, w_recv, wy_send, wy_recv, f_send, f_recv,
    tz_send, tz_recv, tx_send, tx_recv, tt_send, tt_recv,
    oz_send, oz_recv, oy_send, oy_recv,
    h_send, h_recv, s_send, s_recv,
    jz_send, jz_recv, l_send, l_recv, jx_send, jx_recv, jt_send, jt_recv,
):
    Z, Y, TP, TC, OC = sizes
    XH = TP // 2
    R, D = tokens.shape
    N = R * TP
    KD, C = packed.shape[1:]
    KO = w_out.shape[0]
    RC, RO = R // TC, KO // OC
    S = Z * Y
    sp, tp = lax.axis_index("sp"), lax.axis_index("tp")
    z, y = sp // Y, sp % Y
    twin = tp + 1 - 2 * (tp % 2)
    can_up, can_down = z < Z - 1, z > 0

    def remote(src, dst, send, recv, to_sp, to_tp):
        return pltpu.make_async_remote_copy(
            src_ref=src, dst_ref=dst, send_sem=send, recv_sem=recv,
            device_id={"sp": to_sp, "tp": to_tp}, device_id_type=MESH,
        )

    def side_tp(k):
        return (tp + 2 * k) % TP

    def from_tp(k):
        return (tp + TP - 2 * k) % TP

    def up_z(k):
        return (z + k) % Z

    def back_z(k):
        return (z + Z - k) % Z

    def up_y(k):
        return (y + k) % Y

    def back_y(k):
        return (y + Y - k) % Y

    def w_rows(zz, yy):
        return W.at[pl.ds(pl.multiple_of((zz * Y + yy) * KD, KD), KD), :]

    def w_across(k, source):
        return remote(
            packed.at[up_z(k)], w_rows(source, y), w_send.at[k], w_recv.at[k], up_z(k) * Y + y, tp
        )

    def w_side(k, j, source):
        zz = back_z(k)
        src = packed.at[z] if k == 0 else w_rows(zz, y)
        return remote(
            src, w_rows(zz, source), wy_send.at[k, j - 1], wy_recv.at[k, j - 1], z * Y + up_y(j), tp
        )

    def f_across(k, source):
        return remote(
            shifts.at[up_z(k)], FS.at[source], f_send.at[k], f_recv.at[k], up_z(k) * Y + y, tp
        )

    def t_rows(zz, tt, c):
        start = pl.multiple_of((zz * TP + tt) * R + c * RC, RC)
        return T.at[pl.ds(start, RC), :]

    def t_line(zz, way, c):
        place = t_rows(zz, tp, c)
        to = (z + 1 - 2 * way) * Y + y
        return remote(place, place, tz_send.at[way, zz, c], tz_recv.at[zz, c], to, tp)

    def t_side(zz, k, c, source):
        place = t_rows(zz, source, c)
        return remote(place, place, tx_send.at[k - 1, zz, c], tx_recv.at[k - 1, zz, c], sp, side_tp(k))

    def t_twin(zz, k, c, source):
        place = t_rows(zz, source, c)
        return remote(place, place, tt_send.at[k, zz, c], tt_recv.at[k, zz, c], sp, twin)

    def o_rows(zz, yy, c):
        start = pl.multiple_of((zz * Y + yy) * KO + c * RO, RO)
        return O.at[pl.ds(start, RO), :]

    def o_line(zz, way, c, own):
        place = o_rows(zz, y, c)
        src = w_out.at[pl.ds(c * RO, RO), :] if own else place
        to = (z + 1 - 2 * way) * Y + y
        return remote(src, place, oz_send.at[way, zz, c], oz_recv.at[zz, c], to, tp)

    def o_side(zz, k, c, source, own):
        place = o_rows(zz, source, c)
        src = w_out.at[pl.ds(c * RO, RO), :] if own else place
        return remote(src, place, oy_send.at[k - 1, zz, c], oy_recv.at[k - 1, zz, c], z * Y + up_y(k), tp)

    def h_side(zz, shift):
        rows = pl.ds(pl.multiple_of(zz * N + N - WINDOW, WINDOW), WINDOW)
        return remote(
            PROJ.at[rows, pl.ds(3 * LANES, LANES)], HALO.at[zz + shift],
            h_send.at[zz], h_recv.at[zz], z * Y + up_y(1), tp,
        )

    def s_side(zz, k, source):
        place = ST.at[zz * Y + source]
        return remote(place, place, s_send.at[k - 1, zz], s_recv.at[k - 1, zz], z * Y + up_y(k), tp)

    def j_across(k, source):
        return remote(JS.at[up_z(k)], J.at[tp, source], jz_send.at[k], jz_recv.at[k], up_z(k) * Y + y, tp)

    def l_across(k, source):
        return remote(LS.at[up_z(k)], LT.at[source], l_send.at[k], l_recv.at[k], up_z(k) * Y + y, tp)

    def j_side(zz, k, source):
        place = J.at[source, zz]
        return remote(place, place, jx_send.at[k - 1, zz], jx_recv.at[k - 1, zz], sp, side_tp(k))

    def j_twin(zz, k, source):
        place = J.at[source, zz]
        return remote(place, place, jt_send.at[k, zz], jt_recv.at[k, zz], sp, twin)

    keep = [
        pltpu.make_async_copy(packed.at[z], w_rows(z, y), own_sems.at[0]),
        pltpu.make_async_copy(gate_cols, GW, own_sems.at[1]),
        pltpu.make_async_copy(
            w_out, O.at[pl.ds(pl.multiple_of(sp * KO, KO), KO), :], own_sems.at[2]
        ),
    ]

    barrier = pltpu.get_barrier_semaphore()
    greeted = [(up_z(k) * Y + y, tp) for k in range(1, Z)]
    greeted += [(z * Y + up_y(k), tp) for k in range(1, Y)]
    greeted += [(sp, side_tp(k)) for k in range(1, XH)] + [(sp, twin)]
    for to_sp, to_tp in greeted:
        pl.semaphore_signal(
            barrier, inc=1, device_id={"sp": to_sp, "tp": to_tp}, device_id_type=MESH
        )
    for copy in keep:
        copy.start()

    step = 16
    for i in range(R // step):
        values = tokens[pl.ds(i * step, step), :].astype(jnp.float32)
        rescale = lax.rsqrt(jnp.mean(values * values, axis=-1, keepdims=True) + EPSILON)
        start = pl.multiple_of((z * TP + tp) * R + i * step, step)
        T[pl.ds(start, step), :] = (values * rescale * gain[...]).astype(jnp.bfloat16)
    FS[z] = shifts[z]

    @pl.when(y == 0)
    def _():
        HALO[0] = jnp.zeros(HALO.shape[1:], HALO.dtype)

    pl.semaphore_wait(barrier, len(greeted))

    def weights_out(act):
        for k in range(1, Z):
            act(w_across(k, z))
            act(f_across(k, z))
        for j in range(1, Y):
            act(w_side(0, j, y))

    def own_tokens(act):
        for c in range(TC):
            pl.when(can_up)(lambda: act(t_line(z, 0, c)))
            pl.when(can_down)(lambda: act(t_line(z, 1, c)))
            for k in range(1, XH):
                act(t_side(z, k, c, tp))
            act(t_twin(z, 0, c, tp))

    def weights_on(act):
        for k in range(1, Z):
            if act is begin:
                w_across(k, back_z(k)).wait_recv()
            for j in range(1, Y):
                act(w_side(k, j, y))

    def tokens_on(d, act):
        for way, origin, there, further in (
            (0, z - d, z - d >= 0, can_up), (1, z + d, z + d < Z, can_down),
        ):
            def landed(way=way, origin=origin, further=further):
                for c in range(TC):
                    if act is begin:
                        t_line(origin, way, c).wait_recv()
                    pl.when(further)(lambda: act(t_line(origin, way, c)))
                    for k in range(1, XH):
                        act(t_side(origin, k, c, tp))
                    act(t_twin(origin, 0, c, tp))

            pl.when(there)(landed)

    def tokens_aside(zz, act):
        for k in range(1, XH):
            for c in range(TC):
                if act is begin:
                    t_side(zz, k, c, from_tp(k)).wait_recv()
                act(t_twin(zz, k, c, from_tp(k)))

    def own_output(act):
        for c in range(OC):
            pl.when(can_up)(lambda: act(o_line(z, 0, c, True)))
            pl.when(can_down)(lambda: act(o_line(z, 1, c, True)))
            for k in range(1, Y):
                act(o_side(z, k, c, y, True))

    def output_on(d, act):
        for way, origin, there, further in (
            (0, z - d, z - d >= 0, can_up), (1, z + d, z + d < Z, can_down),
        ):
            def landed(way=way, origin=origin, further=further):
                for c in range(OC):
                    if act is begin:
                        o_line(origin, way, c, False).wait_recv()
                    pl.when(further)(lambda: act(o_line(origin, way, c, False)))
                    for k in range(1, Y):
                        act(o_side(origin, k, c, y, False))

            pl.when(there)(landed)

    def block_rows(zz):
        return pl.ds(pl.multiple_of(zz * N, N), N)

    depth = 1024

    def project(zz):
        ACC[...] = jnp.zeros_like(ACC)

        def part(i, nothing):
            cols = pl.ds(pl.multiple_of(i * depth, depth), depth)
            block = T[block_rows(zz), cols]
            ACC[:, :C] += dot(block, W[cols, :])
            ACC[:, C:] += dot(block, GW[cols, :])
            return nothing

        lax.fori_loop(0, D // depth, part, 0)
        PROJ[block_rows(zz), :] = ACC[:, :C].astype(jnp.bfloat16)

    parts = N // WINDOW
    wide = (WINDOW, LANES)

    def sub_rows(zz, i):
        return pl.ds(pl.multiple_of(zz * N + i * WINDOW, WINDOW), WINDOW)

    def attend(zz, i, before):
        lane = lanes_of(wide)
        heads = PROJ[sub_rows(zz, i), :LANES].astype(jnp.float32) * HD ** (-0.5)
        first = jnp.where(lane < HD, heads, 0.0)
        second = jnp.where(lane < HD, pltpu.roll(heads, HD, 1), 0.0)
        query = jnp.concatenate([first, second], axis=0).astype(jnp.bfloat16)
        rows = jnp.concatenate([before, PROJ[sub_rows(zz, i), 3 * LANES :]], axis=0)
        scores = lax.dot_general(
            query, rows, (((1,), (1,)), ((), ())), preferred_element_type=jnp.float32
        )
        shape = (2 * WINDOW, 2 * WINDOW)
        at = lax.broadcasted_iota(jnp.int32, shape, 0)
        head = at >= WINDOW
        key_at = lax.broadcasted_iota(jnp.int32, shape, 1)
        distance = jnp.where(head, at - WINDOW, at) - key_at + WINDOW
        allowed = (distance >= 0) & (distance < WINDOW)
        if i == 0:
            lowest = WINDOW * (1 - jnp.minimum(zz * Y + y, 1))
            allowed = allowed & (key_at >= lowest)
        scores = jnp.where(allowed, scores, MASKED)
        tall = lax.broadcasted_iota(jnp.int32, (2 * WINDOW, 1), 0) >= WINDOW
        sink = jnp.where(tall, sinks[2 * z + 1], sinks[2 * z])
        ceiling = jnp.maximum(jnp.max(scores, axis=-1, keepdims=True), sink)
        weights = jnp.exp(scores - ceiling)
        total = jnp.exp(sink - ceiling) + jnp.sum(weights, axis=-1, keepdims=True)
        probs = (weights * (1.0 / total)).astype(jnp.bfloat16)
        out = dot(probs, rows)
        both = jnp.where(lane < HD, pltpu.roll(out[:WINDOW], HD, 1), out[WINDOW:])
        JS[zz, pl.ds(i * WINDOW, WINDOW), :] = both.astype(jnp.bfloat16)
        logs = jnp.broadcast_to(ceiling + jnp.log(total), (2 * WINDOW, LANES)).T
        LS[zz, 0:1, pl.ds(i * WINDOW, WINDOW)] = logs[0:1, :WINDOW]
        LS[zz, 1:2, pl.ds(i * WINDOW, WINDOW)] = logs[0:1, WINDOW:]

    def remember(zz):
        flat = ACC[:, C:].T
        log_in = flat[0:1, :] - 0.5 * math.log(N * S)
        pre = flat[1:2, :] + bias[z]
        log_sig = jnp.minimum(pre, 0.0) - jnp.log1p(jnp.exp(-jnp.abs(pre)))
        log_forget = log_sig + FS[zz][0:1, :]
        square = (N, N)
        before = lax.broadcasted_iota(jnp.int32, square, 0) <= lax.broadcasted_iota(
            jnp.int32, square, 1
        )
        summed = dot(
            jnp.broadcast_to(log_forget, (8, N)), before.astype(jnp.float32),
            precision=lax.Precision.HIGHEST,
        )[0:1, :]
        passed = summed[:, N - 1 :]
        decays = passed - summed + log_in
        level = jnp.max(decays, axis=1, keepdims=True)
        weights = jnp.exp(decays - level)
        pair = PROJ[block_rows(zz), LANES : 2 * LANES].astype(jnp.float32)
        query = (pair[:, :HD] * HD ** (-0.5)).astype(jnp.bfloat16)
        keys = pair.T[HD:, :]
        lane = lanes_of((N, LANES))
        values = PROJ[block_rows(zz), 2 * LANES : 3 * LANES].astype(jnp.float32)
        values = jnp.where(lane < HD, values, jnp.where(lane == HD, 1.0, 0.0)).astype(jnp.bfloat16)
        state = dot((keys * weights).astype(jnp.bfloat16), values)
        lane = lanes_of(state.shape)
        state = jnp.where(lane == HD + 1, passed, jnp.where(lane == HD + 2, level, state))
        ST[zz * Y + y] = state
        for k in range(1, Y):
            s_side(zz, k, y).start()
        keys = keys.astype(jnp.bfloat16)
        summed_col = jnp.broadcast_to(summed, (LANES, N)).T
        source = log_in - summed
        lane = lanes_of(wide)
        for i in range(parts):
            width = (i + 1) * WINDOW
            span = (WINDOW, width)
            causal = lax.broadcasted_iota(jnp.int32, span, 0) + i * WINDOW >= lanes_of(span)
            since = summed_col[i * WINDOW : (i + 1) * WINDOW, :]
            log_weight = jnp.where(causal, since[:, :1] + source[:, :width], MASKED)
            peak = jnp.max(log_weight, axis=-1, keepdims=True)
            affinity = dot(query[i * WINDOW : (i + 1) * WINDOW], keys[:, :width]) * jnp.exp(
                log_weight - peak
            )
            total = jnp.sum(affinity, axis=-1, keepdims=True)
            found = dot(affinity.astype(jnp.bfloat16), values[:width])
            NUM[sub_rows(zz, i), :] = jnp.where(
                lane < HD, found,
                jnp.where(lane == HD, total, jnp.where(lane == HD + 1, peak, since)),
            )

    def local_work(zz):
        project(zz)
        h_side(zz, (y + 1) // Y).start()
        remember(zz)
        for i in range(1, parts):
            attend(zz, i, PROJ[sub_rows(zz, i - 1), 3 * LANES :])

    weights_out(begin)
    own_tokens(begin)
    weights_on(begin)
    for k in range(1, Z):
        f_across(k, back_z(k)).wait_recv()
    for k in range(Z):
        for j in range(1, Y):
            w_side(k, j, back_y(j)).wait_recv()
    keep[0].wait()
    keep[1].wait()

    def stage(i, nothing):
        @pl.when(i == 1)
        def _():
            tokens_on(1, begin)

        @pl.when((i >= 1) & (i + 1 < Z))
        def _():
            tokens_on(i + 1, begin)

        @pl.when(i == Z - 1)
        def _():
            own_output(begin)

        def one(side, nothing):
            zz = z + i * (2 * side - 1)

            @pl.when((zz >= 0) & (zz < Z) & (i + 1 - side > 0))
            def _():
                tokens_aside(zz, begin)
                for k in range(XH):
                    for c in range(TC):
                        t_twin(zz, k, c, (twin + TP - 2 * k) % TP).wait_recv()
                local_work(zz)

            return nothing

        lax.fori_loop(0, 2, one, 0)
        return nothing

    lax.fori_loop(0, Z, stage, 0)

    output_on(1, begin)

    for zz in range(Z):
        h_side(zz, 1 - jnp.minimum(y, 1)).wait_recv()
        for k in range(1, Y):
            s_side(zz, k, back_y(k)).wait_recv()

    def enter():
        carried = jnp.zeros((HD, LANES), jnp.float32)
        stabilizer = jnp.full((1, 1), MASKED, jnp.float32)
        lane = lanes_of((HD, LANES))
        for i in range(S):
            @pl.when(y == i % Y)
            def _(carried=carried, stabilizer=stabilizer):
                EB[i // Y] = jnp.where(lane == HD + 1, stabilizer, carried)

            state = ST[i]
            passed, level = state[0:1, HD + 1 : HD + 2], state[0:1, HD + 2 : HD + 3]
            newer = jnp.maximum(stabilizer + passed, level)
            carried = carried * jnp.exp(stabilizer + passed - newer) + state * jnp.exp(level - newer)
            stabilizer = newer

    enter()

    def finish(zz):
        attend(zz, 0, HALO[zz])
        entering = EB[zz]
        stabilizer = entering[0:1, HD + 1 : HD + 2]
        local = NUM[block_rows(zz), :]
        peak, since = local[:, HD + 1 : HD + 2], local[:, HD + 2 : HD + 3]
        pair = PROJ[block_rows(zz), LANES : 2 * LANES].astype(jnp.float32)
        query = (pair[:, :HD] * HD ** (-0.5)).astype(jnp.bfloat16)
        carried = dot(query, entering.astype(jnp.bfloat16))
        older = since + stabilizer
        row_level = jnp.maximum(older, peak)
        found = jnp.exp(older - row_level) * carried + jnp.exp(peak - row_level) * local
        bound = jnp.maximum(jnp.abs(found[:, HD : HD + 1]), jnp.exp(-row_level))
        gate = pltpu.roll(
            PROJ[block_rows(zz), 2 * LANES : 3 * LANES].astype(jnp.float32), HD, 1
        )
        recall = found / bound * jax.nn.sigmoid(gate)
        half = N // 2
        lane = lanes_of((half, LANES))
        paired = jnp.where(lane < HD, recall[:half], pltpu.roll(recall[half:], HD, 1))
        JS[zz, N:, :] = paired.astype(jnp.bfloat16)

    def hand_over(act):
        for k in range(1, Z):
            act(j_across(k, z))
            act(l_across(k, z))

    for k in range(1, Z):
        finish(up_z(k))
        j_across(k, z).start()
        l_across(k, z).start()
        if k > 1:
            output_on(k, begin)
    finish(z)
    J[tp, z] = JS[z]
    LT[z] = LS[z]

    def share(act):
        for k in range(Z):
            zz = back_z(k)
            if k and act is begin:
                j_across(k, zz).wait_recv()
            for j in range(1, XH):
                act(j_side(zz, j, tp))
            act(j_twin(zz, 0, tp))
        for k in range(Z):
            zz = back_z(k)
            for j in range(1, XH):
                if act is begin:
                    j_side(zz, j, from_tp(j)).wait_recv()
                act(j_twin(zz, j, from_tp(j)))

    share(begin)
    for k in range(1, Z):
        l_across(k, back_z(k)).wait_recv()
    for k in range(XH):
        for zz in range(Z):
            j_twin(zz, k, (twin + TP - 2 * k) % TP).wait_recv()

    mem_base = TP * sinks.shape[0] * HD
    per_tp = sinks.shape[0] * HD
    half = N // 2
    LTF[...] = jnp.zeros_like(LTF)
    for zz in range(Z):
        for t in range(TP):
            at = t * per_tp + zz * LANES
            X[:, at : at + LANES] = J[t, zz, :N, :]
            at = mem_base + (t * Z + zz) * HD
            X[:half, at : at + HD] = J[t, zz, N:, :HD]
            X[half:, at : at + HD] = J[t, zz, N:, HD:]
        LTF[2 * zz : 2 * zz + 2, :] = LT[zz, 0:2, :]
    totals[...] = LTF[...].T[:, : sinks.shape[0]]

    keep[2].wait()
    for zz in range(Z):
        for k in range(1, Y):
            for c in range(OC):
                o_side(zz, k, c, back_y(k), False).wait_recv()

    tile = 256

    def columns(i, nothing):
        cols = pl.ds(pl.multiple_of(i * tile, tile), tile)
        mixed[:, cols] = dot(X[...], O[:, cols]).astype(jnp.bfloat16)
        return nothing

    lax.fori_loop(0, mixed.shape[1] // tile, columns, 0)

    weights_out(drain)
    own_tokens(drain)
    weights_on(drain)
    own_output(drain)

    def settle(i, nothing):
        tokens_on(i, drain)
        output_on(i, drain)
        return nothing

    lax.fori_loop(1, Z, settle, 0)
    for zz in range(Z):
        tokens_aside(zz, drain)
        h_side(zz, (y + 1) // Y).wait_send()
        for k in range(1, Y):
            s_side(zz, k, y).wait_send()
    hand_over(drain)
    share(drain)


def mix(tokens, gain, packed, shifts, gate_cols, w_out, sinks, bias):
    S, TP = lax.axis_size("sp"), lax.axis_size("tp")
    Z = packed.shape[0]
    Y, XH = S // Z, TP // 2
    R, D = tokens.shape
    N = R * TP
    C = packed.shape[2]
    TC = OC = 3
    M = w_out.shape[1]
    bf, f32 = jnp.bfloat16, jnp.float32
    dma = pltpu.SemaphoreType.DMA
    piece = N + N // 2
    vmem = pl.BlockSpec(memory_space=pltpu.VMEM)
    smem = pl.BlockSpec(memory_space=pltpu.SMEM)
    hbm = pl.BlockSpec(memory_space=pl.ANY)
    return pl.pallas_call(
        functools.partial(mixer_kernel, (Z, Y, TP, TC, OC)),
        out_shape=[
            jax.ShapeDtypeStruct((N, M), bf),
            jax.ShapeDtypeStruct((N, sinks.shape[0]), f32),
        ],
        in_specs=[vmem, vmem, hbm, vmem, hbm, hbm, smem, smem],
        out_specs=[vmem, vmem],
        scratch_shapes=[
            pltpu.VMEM((Z * N, D), bf),
            pltpu.VMEM((D, C), bf),
            pltpu.VMEM((D, LANES), bf),
            pltpu.VMEM((S * w_out.shape[0], M), bf),
            pltpu.VMEM((N, C + LANES), f32),
            pltpu.VMEM((Z * N, C), bf),
            pltpu.VMEM((Z * N, LANES), f32),
            pltpu.VMEM((S, HD, LANES), f32),
            pltpu.VMEM((Z, HD, LANES), f32),
            pltpu.VMEM((Z + 1, WINDOW, LANES), bf),
            pltpu.VMEM((Z, 8, N), f32),
            pltpu.VMEM((Z, piece, LANES), bf),
            pltpu.VMEM((TP, Z, piece, LANES), bf),
            pltpu.VMEM((Z, 8, N), f32),
            pltpu.VMEM((Z, 8, N), f32),
            pltpu.VMEM((LANES, N), f32),
            pltpu.VMEM((N, S * w_out.shape[0]), bf),
            dma((3,)),
            dma((Z,)), dma((Z,)), dma((Z, Y - 1)), dma((Z, Y - 1)), dma((Z,)), dma((Z,)),
            dma((2, Z, TC)), dma((Z, TC)), dma((XH - 1, Z, TC)), dma((XH - 1, Z, TC)),
            dma((XH, Z, TC)), dma((XH, Z, TC)),
            dma((2, Z, OC)), dma((Z, OC)), dma((Y - 1, Z, OC)), dma((Y - 1, Z, OC)),
            dma((Z,)), dma((Z,)), dma((Y - 1, Z)), dma((Y - 1, Z)),
            dma((Z,)), dma((Z,)), dma((Z,)), dma((Z,)),
            dma((XH - 1, Z)), dma((XH - 1, Z)), dma((XH, Z)), dma((XH, Z)),
        ],
        compiler_params=pltpu.CompilerParams(
            collective_id=0, has_side_effects=True, vmem_limit_bytes=60 * 2**20
        ),
    )(tokens, gain, packed, shifts, gate_cols, w_out, sinks, bias)


def shards(
    tokens,
    norm_gain,
    w_query,
    w_key,
    w_value,
    w_mem_query,
    w_mem_key,
    w_mem_value,
    w_mem_gate,
    w_gates,
    sinks,
    forget_bias,
    forget_shift,
    w_out,
):
    mem_heads = forget_bias.shape[0]
    Z = mem_heads
    Y = lax.axis_size("sp") // Z
    z, tp = lax.axis_index("sp") // Y, lax.axis_index("tp")
    q_width = w_query.shape[1] // Z
    per_z = q_width // HD
    group = w_query.shape[1] // w_key.shape[1]

    def piece(i):
        kv = i * per_z // group * HD
        mem = [
            part[:, i * HD : (i + 1) * HD]
            for part in (w_mem_query, w_mem_key, w_mem_value, w_mem_gate)
        ]
        return jnp.concatenate(
            [w_query[:, i * q_width : (i + 1) * q_width]]
            + mem
            + [w_key[:, kv : kv + HD], w_value[:, kv : kv + HD]],
            axis=1,
        )

    packed = jnp.stack([piece(i) for i in range(Z)])
    head = tp * mem_heads + z
    gate_cols = lax.dynamic_slice_in_dim(w_gates, head, 1, 2)[:, :, 0]
    gate_cols = jnp.pad(gate_cols, ((0, 0), (0, LANES - 2)))
    shifts = jnp.pad(forget_shift.T[:, None, :], ((0, 0), (0, 7), (0, 0)))
    mixed, totals = mix(
        tokens, norm_gain[None, :], packed, shifts, gate_cols, w_out, sinks, forget_bias
    )
    return mixed, totals


def solution(mesh):
    placed = (
        P(("sp", "tp"), None),
        P(),
        P("sp", "tp"),
        P("sp", "tp"),
        P("sp", "tp"),
        P("sp", "tp"),
        P("sp", "tp"),
        P("sp", "tp"),
        P("sp", "tp"),
        P(),
        P("tp"),
        P("tp"),
        P("sp", "tp"),
        P("sp", "tp"),
    )
    return jax.shard_map(
        shards,
        mesh=mesh,
        in_specs=placed,
        out_specs=(P("sp", "tp"), P("sp", "tp")),
        check_vma=False,
    )
```

profile of v0, /device:TPU:0, one launch (start us, length us, event | category | flops | bytes accessed | tf_op | source)
XLA Modules:
  0.0 226.2 jit_solution(3239522826853067215)
XLA Ops:
  0.6 0.0 copy-start
  0.6 0.0 copy-start.2
  0.7 0.0 copy-start.1
  0.7 0.0 copy-start.5
  0.7 0.0 copy-start.4
  0.7 1.6 fusion.3
  2.3 0.0 copy-start.3
  2.3 0.0 copy-done.2
  2.3 0.0 copy-done.1
  2.3 0.2 fusion.1
  2.6 0.0 copy-done.5
  2.6 0.0 copy-done.4
  2.6 0.1 fusion.5
  2.7 0.6 copy-done.3
  3.3 0.8 fusion
  4.1 1.2 concatenate.12
  5.3 1.2 concatenate.13
  6.5 1.2 concatenate.14
  7.6 0.4 concatenate.15
  8.1 1.6 pad_maximum_fusion.packed
  9.7 0.0 copy-start.6
  9.7 0.0 copy-done
  9.7 0.5 copy.16
  10.2 1.2 pad.9.gate_cols
  11.4 0.0 copy-done.6
  11.4 0.6 pad.8.shifts
  12.1 210.4 %shard_map.149 = (bf16[384,1024]{1,0:T(8,128)(2,1)}, f32[384,8]{1,0:T(8,128)}) custom-call(bf16[96,4096]{1,0:T(8,128)(2,1)} %tokens.1, f32[1,4096]{1,0:T(1,128)} %bitcast.12, bf16[4,512,512]{2,1,0:T(8,128)(2,1)} %pad_maximum_fusion.packed, f32[4,8,384]{2,1,0:T(8,128)} %pad.8.shifts, bf16[4096,128]{1,0:T(8,128)(2,1)} %pad.9.gate_cols, ...), custom_call_target="tpu_custom_call" | custom-call | tf_op jit(solution)/shard_map/pallas_call | solution.py:562
  222.5 1.6 copy.17
  224.1 2.1 copy.19
  (2 shorter events, 0.0 us)
Async XLA Ops:
  0.6 9.0 %copy-start = (bf16[4096,2,16]{0,2,1:T(8,128)(2,1)S(1)}, bf16[4096,2,16]{0,2,1:T(8,128)(2,1)}, u32[]{:S(2)}) copy-start(bf16[4096,2,16]{0,2,1:T(8,128)(2,1)} %param.23) | copy-start | bytes 786436
  0.6 1.6 copy-start.2
  0.7 1.6 copy-start.1
  0.7 1.9 copy-start.5
  0.7 1.9 copy-start.4
  2.3 1.0 copy-start.3
  9.7 1.8 copy-start.6
where the time goes:
time: 228 us; the launch traced here: 226 us
  Pallas kernels  210 us (92%)
  local copies, waits for them, and re-layouts  13.4 us (6%)
    pallas_call x1, Pallas kernels, mix(): pl.pallas_call(functools.partial(mixer_kernel, (Z, Y, TP, TC, OC)), out_s...  210 us

commit v1 on v0

--- a/solution.py
+++ b/solution.py
@@ -34,22 +34,24 @@
 
 def mixer_kernel(
     sizes,
-    tokens, gain, packed, shifts, gate_cols, w_out, sinks, bias,
+    tokens, gain, shifts, gates, w_out, w_query, w_key, w_value, w_mem_query, w_mem_key,
+    w_mem_value, w_mem_gate, sinks, bias,
     mixed, totals,
-    T, W, GW, O, ACC, PROJ, NUM, ST, EB, HALO, FS, JS, J, LS, LT, LTF, X,
+    in_query, in_key, in_value, in_mem_query, in_mem_key, in_mem_value, in_mem_gate,
+    PACK, T, W, GW, O, ACC, FLAT, PROJ, NUM, ST, EB, HALO, SH, FS, JS, J, LS, LT, X,
     own_sems, w_send, w_recv, wy_send, wy_recv, f_send, f_recv,
     tz_send, tz_recv, tx_send, tx_recv, tt_send, tt_recv,
     oz_send, oz_recv, oy_send, oy_recv,
     h_send, h_recv, s_send, s_recv,
     jz_send, jz_recv, l_send, l_recv, jx_send, jx_recv, jt_send, jt_recv,
 ):
-    Z, Y, TP, TC, OC = sizes
+    Z, Y, TP, TC, WC, OC = sizes
     XH = TP // 2
     R, D = tokens.shape
     N = R * TP
-    KD, C = packed.shape[1:]
+    KD, C = PACK.shape[1:]
     KO = w_out.shape[0]
-    RC, RO = R // TC, KO // OC
+    RC, RW, RO = R // TC, KD // WC, KO // OC
     S = Z * Y
     sp, tp = lax.axis_index("sp"), lax.axis_index("tp")
     z, y = sp // Y, sp % Y
@@ -80,24 +82,32 @@
     def back_y(k):
         return (y + Y - k) % Y
 
-    def w_rows(zz, yy):
-        return W.at[pl.ds(pl.multiple_of((zz * Y + yy) * KD, KD), KD), :]
-
-    def w_across(k, source):
+    def w_rows(zz, yy, c):
+        return W.at[pl.ds(pl.multiple_of((zz * Y + yy) * KD + c * RW, RW), RW), :]
+
+    def w_across(way, d, c):
+        to = z + d * (1 - 2 * way)
         return remote(
-            packed.at[up_z(k)], w_rows(source, y), w_send.at[k], w_recv.at[k], up_z(k) * Y + y, tp
-        )
-
-    def w_side(k, j, source):
-        zz = back_z(k)
-        src = packed.at[z] if k == 0 else w_rows(zz, y)
+            PACK.at[to, pl.ds(c * RW, RW), :], w_rows(z, y, c),
+            w_send.at[way, d, c], w_recv.at[way, d, c], to * Y + y, tp,
+        )
+
+    def w_landed(way, d, c):
+        origin = z - d * (1 - 2 * way)
         return remote(
-            src, w_rows(zz, source), wy_send.at[k, j - 1], wy_recv.at[k, j - 1], z * Y + up_y(j), tp
+            PACK.at[z, pl.ds(c * RW, RW), :], w_rows(origin, y, c),
+            w_send.at[way, d, c], w_recv.at[way, d, c], sp, tp,
+        )
+
+    def w_side(zz, j, c, source):
+        place = w_rows(zz, source, c)
+        return remote(
+            place, place, wy_send.at[j - 1, zz, c], wy_recv.at[j - 1, zz, c], z * Y + up_y(j), tp
         )
 
     def f_across(k, source):
         return remote(
-            shifts.at[up_z(k)], FS.at[source], f_send.at[k], f_recv.at[k], up_z(k) * Y + y, tp
+            SH.at[up_z(k)], FS.at[source], f_send.at[k], f_recv.at[k], up_z(k) * Y + y, tp
         )
 
     def t_rows(zz, tt, c):
@@ -157,13 +167,12 @@
         place = J.at[source, zz]
         return remote(place, place, jt_send.at[k, zz], jt_recv.at[k, zz], sp, twin)
 
-    keep = [
-        pltpu.make_async_copy(packed.at[z], w_rows(z, y), own_sems.at[0]),
-        pltpu.make_async_copy(gate_cols, GW, own_sems.at[1]),
-        pltpu.make_async_copy(
-            w_out, O.at[pl.ds(pl.multiple_of(sp * KO, KO), KO), :], own_sems.at[2]
-        ),
-    ]
+    ins = (
+        (w_query, in_query), (w_key, in_key), (w_value, in_value), (w_mem_query, in_mem_query),
+        (w_mem_key, in_mem_key), (w_mem_value, in_mem_value), (w_mem_gate, in_mem_gate),
+        (gates, GW), (w_out, O.at[pl.ds(pl.multiple_of(sp * KO, KO), KO), :]),
+    )
+    keep = [pltpu.make_async_copy(a, b, own_sems.at[i]) for i, (a, b) in enumerate(ins)]
 
     barrier = pltpu.get_barrier_semaphore()
     greeted = [(up_z(k) * Y + y, tp) for k in range(1, Z)]
@@ -182,20 +191,76 @@
         rescale = lax.rsqrt(jnp.mean(values * values, axis=-1, keepdims=True) + EPSILON)
         start = pl.multiple_of((z * TP + tp) * R + i * step, step)
         T[pl.ds(start, step), :] = (values * rescale * gain[...]).astype(jnp.bfloat16)
-    FS[z] = shifts[z]
+    for i in range(Z):
+        SH[i, 0:1, :] = shifts[i : i + 1, :]
+    FS[z] = SH[z]
 
     @pl.when(y == 0)
     def _():
         HALO[0] = jnp.zeros(HALO.shape[1:], HALO.dtype)
 
-    pl.semaphore_wait(barrier, len(greeted))
-
-    def weights_out(act):
-        for k in range(1, Z):
-            act(w_across(k, z))
-            act(f_across(k, z))
-        for j in range(1, Y):
-            act(w_side(0, j, y))
+    with jax.named_scope('barrier_wait'):
+        pl.semaphore_wait(barrier, len(greeted))
+
+    def pack():
+        for copy in keep[:7]:
+            copy.wait()
+        group = w_query.shape[1] // w_key.shape[1]
+        high = min(KD, WINDOW)
+        lane = lanes_of((high, LANES))
+
+        def halves(rows, left, i, right, j):
+            a = left[rows, pl.ds(i // 2 * LANES, LANES)].astype(jnp.float32)
+            b = right[rows, pl.ds(j // 2 * LANES, LANES)].astype(jnp.float32)
+            a = pltpu.roll(a, HD, 1) if i % 2 else a
+            b = b if j % 2 else pltpu.roll(b, HD, 1)
+            return jnp.where(lane < HD, a, b).astype(jnp.bfloat16)
+
+        def some(r, nothing):
+            rows = pl.ds(pl.multiple_of(r * high, high), high)
+            for i in range(Z):
+                kv = i * (LANES // HD) // group
+                PACK[i, rows, :LANES] = in_query[rows, i * LANES : (i + 1) * LANES]
+                for n, parts in enumerate(
+                    (
+                        (in_mem_query, i, in_mem_key, i),
+                        (in_mem_value, i, in_mem_gate, i),
+                        (in_key, kv, in_value, kv),
+                    )
+                ):
+                    PACK[i, rows, (n + 1) * LANES : (n + 2) * LANES] = halves(rows, *parts)
+            return nothing
+
+        lax.fori_loop(0, KD // high, some, 0)
+        W[pl.ds(pl.multiple_of(sp * KD, KD), KD), :] = PACK[z]
+
+    def ways(d):
+        return ((0, z + d < Z, z - d >= 0), (1, z - d >= 0, z + d < Z))
+
+    def weights_out(way, d, act):
+        for c in range(WC):
+            act(w_across(way, d, c))
+
+    def weights_far(act):
+        for d in range(2, Z):
+            for way, there, _ in ways(d):
+                pl.when(there)(lambda: weights_out(way, d, act))
+
+    def weights_aside(zz, act):
+        for c in range(WC):
+            for j in range(1, Y):
+                act(w_side(zz, j, c, y))
+
+    def weights_on(d, act):
+        for way, _, there in ways(d):
+            def landed(way=way):
+                for c in range(WC):
+                    if act is begin:
+                        w_landed(way, d, c).wait_recv()
+                    for j in range(1, Y):
+                        act(w_side(z - d * (1 - 2 * way), j, c, y))
+
+            pl.when(there)(landed)
 
     def own_tokens(act):
         for c in range(TC):
@@ -204,13 +269,6 @@
             for k in range(1, XH):
                 act(t_side(z, k, c, tp))
             act(t_twin(z, 0, c, tp))
-
-    def weights_on(act):
-        for k in range(1, Z):
-            if act is begin:
-                w_across(k, back_z(k)).wait_recv()
-            for j in range(1, Y):
-                act(w_side(k, j, y))
 
     def tokens_on(d, act):
         for way, origin, there, further in (
@@ -234,12 +292,15 @@
                     t_side(zz, k, c, from_tp(k)).wait_recv()
                 act(t_twin(zz, k, c, from_tp(k)))
 
+    def output_aside(act):
+        for c in range(OC):
+            for k in range(1, Y):
+                act(o_side(z, k, c, y, True))
+
     def own_output(act):
         for c in range(OC):
             pl.when(can_up)(lambda: act(o_line(z, 0, c, True)))
             pl.when(can_down)(lambda: act(o_line(z, 1, c, True)))
-            for k in range(1, Y):
-                act(o_side(z, k, c, y, True))
 
     def output_on(d, act):
         for way, origin, there, further in (
@@ -258,20 +319,19 @@
     def block_rows(zz):
         return pl.ds(pl.multiple_of(zz * N, N), N)
 
-    depth = 1024
-
-    def project(zz):
-        ACC[...] = jnp.zeros_like(ACC)
-
-        def part(i, nothing):
-            cols = pl.ds(pl.multiple_of(i * depth, depth), depth)
-            block = T[block_rows(zz), cols]
-            ACC[:, :C] += dot(block, W[cols, :])
-            ACC[:, C:] += dot(block, GW[cols, :])
+    depth = Y * KD
+
+    def project(zk):
+        cols = pl.ds(pl.multiple_of(zk * depth, depth), depth)
+
+        def part(b, nothing):
+            rows = block_rows(b)
+            block = T[rows, cols]
+            ACC[rows, :C] += dot(block, W[cols, :])
+            ACC[rows, C : C + GW.shape[1]] += dot(block, GW[cols, :])
             return nothing
 
-        lax.fori_loop(0, D // depth, part, 0)
-        PROJ[block_rows(zz), :] = ACC[:, :C].astype(jnp.bfloat16)
+        lax.fori_loop(0, Z, part, 0)
 
     parts = N // WINDOW
     wide = (WINDOW, LANES)
@@ -313,9 +373,11 @@
         LS[zz, 1:2, pl.ds(i * WINDOW, WINDOW)] = logs[0:1, WINDOW:]
 
     def remember(zz):
-        flat = ACC[:, C:].T
-        log_in = flat[0:1, :] - 0.5 * math.log(N * S)
-        pre = flat[1:2, :] + bias[z]
+        FLAT[...] = ACC[block_rows(zz), C:].T
+        gate_count = GW.shape[1] // 2
+        head = tp * Z + z
+        log_in = FLAT[pl.ds(head, 1), :] - 0.5 * math.log(N * S)
+        pre = FLAT[pl.ds(gate_count + head, 1), :] + bias[z]
         log_sig = jnp.minimum(pre, 0.0) - jnp.log1p(jnp.exp(-jnp.abs(pre)))
         log_forget = log_sig + FS[zz][0:1, :]
         square = (N, N)
@@ -340,8 +402,6 @@
         lane = lanes_of(state.shape)
         state = jnp.where(lane == HD + 1, passed, jnp.where(lane == HD + 2, level, state))
         ST[zz * Y + y] = state
-        for k in range(1, Y):
-            s_side(zz, k, y).start()
         keys = keys.astype(jnp.bfloat16)
         summed_col = jnp.broadcast_to(summed, (LANES, N)).T
         source = log_in - summed
@@ -364,60 +424,90 @@
             )
 
     def local_work(zz):
-        project(zz)
+        PROJ[block_rows(zz), :] = ACC[block_rows(zz), :C].astype(jnp.bfloat16)
+        with jax.named_scope('remember'):
+            remember(zz)
         h_side(zz, (y + 1) // Y).start()
-        remember(zz)
-        for i in range(1, parts):
-            attend(zz, i, PROJ[sub_rows(zz, i - 1), 3 * LANES :])
-
-    weights_out(begin)
+        with jax.named_scope('attend'):
+            for i in range(1, parts):
+                attend(zz, i, PROJ[sub_rows(zz, i - 1), 3 * LANES :])
+        for k in range(1, Y):
+            s_side(zz, k, y).start()
+
     own_tokens(begin)
-    weights_on(begin)
+    with jax.named_scope('pack'):
+        pack()
+    for k in range(1, Z):
+        f_across(k, z).start()
+    weights_aside(z, begin)
+    output_aside(begin)
+    ACC[...] = jnp.zeros_like(ACC)
+
+    def both_sides(d, act):
+        def one(side, nothing):
+            zz = z + d * (2 * side - 1)
+            pl.when((zz >= 0) & (zz < Z) & (d + 1 - side > 0))(lambda: act(zz))
+            return nothing
+
+        lax.fori_loop(0, 2, one, 0)
+
+    def near(d, act):
+        pl.when((z == d - 1) & can_up)(lambda: weights_out(0, 1, act))
+        pl.when((z == Z - d) & can_down)(lambda: weights_out(1, 1, act))
+
+    def stage(d, nothing):
+        near(d, begin)
+        with jax.named_scope('t_on'):
+            tokens_on(d, begin)
+        with jax.named_scope('t_aside'):
+            both_sides(d - 1, lambda zz: tokens_aside(zz, begin))
+        return nothing
+
+    lax.fori_loop(1, Z, stage, 0)
+    weights_far(begin)
+    own_output(begin)
+    with jax.named_scope('w_on_1'):
+        weights_on(1, begin)
+    with jax.named_scope('t_last'):
+        both_sides(Z - 1, lambda zz: tokens_aside(zz, begin))
+        for zz in range(Z):
+            for k in range(XH):
+                for c in range(TC):
+                    t_twin(zz, k, c, (twin + TP - 2 * k) % TP).wait_recv()
+    keep[7].wait()
+
+    def multiply(zz):
+        with jax.named_scope('w_side'):
+            for j in range(1, Y):
+                for c in range(WC):
+                    w_side(zz, j, c, back_y(j)).wait_recv()
+        with jax.named_scope('project'):
+            project(zz)
+
+    def stage_two(d, nothing):
+        @pl.when((d > 0) & (d + 1 < Z))
+        def _():
+            with jax.named_scope('w_on'):
+                weights_on(d + 1, begin)
+
+        both_sides(d, multiply)
+        return nothing
+
+    lax.fori_loop(0, Z, stage_two, 0)
     for k in range(1, Z):
         f_across(k, back_z(k)).wait_recv()
-    for k in range(Z):
-        for j in range(1, Y):
-            w_side(k, j, back_y(j)).wait_recv()
-    keep[0].wait()
-    keep[1].wait()
-
-    def stage(i, nothing):
-        @pl.when(i == 1)
-        def _():
-            tokens_on(1, begin)
-
-        @pl.when((i >= 1) & (i + 1 < Z))
-        def _():
-            tokens_on(i + 1, begin)
-
-        @pl.when(i == Z - 1)
-        def _():
-            own_output(begin)
-
-        def one(side, nothing):
-            zz = z + i * (2 * side - 1)
-
-            @pl.when((zz >= 0) & (zz < Z) & (i + 1 - side > 0))
-            def _():
-                tokens_aside(zz, begin)
-                for k in range(XH):
-                    for c in range(TC):
-                        t_twin(zz, k, c, (twin + TP - 2 * k) % TP).wait_recv()
-                local_work(zz)
-
-            return nothing
-
-        lax.fori_loop(0, 2, one, 0)
+
+    def local(zz, nothing):
+        local_work(zz)
         return nothing
 
-    lax.fori_loop(0, Z, stage, 0)
-
-    output_on(1, begin)
-
-    for zz in range(Z):
-        h_side(zz, 1 - jnp.minimum(y, 1)).wait_recv()
-        for k in range(1, Y):
-            s_side(zz, k, back_y(k)).wait_recv()
+    lax.fori_loop(0, Z, local, 0)
+
+    with jax.named_scope('halo_state'):
+        for zz in range(Z):
+            h_side(zz, 1 - jnp.minimum(y, 1)).wait_recv()
+            for k in range(1, Y):
+                s_side(zz, k, back_y(k)).wait_recv()
 
     def enter():
         carried = jnp.zeros((HD, LANES), jnp.float32)
@@ -464,12 +554,12 @@
             act(l_across(k, z))
 
     for k in range(1, Z):
-        finish(up_z(k))
+        with jax.named_scope('finish'):
+            finish(up_z(k))
         j_across(k, z).start()
         l_across(k, z).start()
-        if k > 1:
-            output_on(k, begin)
-    finish(z)
+    with jax.named_scope('finish'):
+        finish(z)
     J[tp, z] = JS[z]
     LT[z] = LS[z]
 
@@ -481,6 +571,8 @@
             for j in range(1, XH):
                 act(j_side(zz, j, tp))
             act(j_twin(zz, 0, tp))
+
+    def share_aside(act):
         for k in range(Z):
             zz = back_z(k)
             for j in range(1, XH):
@@ -488,17 +580,27 @@
                     j_side(zz, j, from_tp(j)).wait_recv()
                 act(j_twin(zz, j, from_tp(j)))
 
-    share(begin)
-    for k in range(1, Z):
-        l_across(k, back_z(k)).wait_recv()
-    for k in range(XH):
-        for zz in range(Z):
-            j_twin(zz, k, (twin + TP - 2 * k) % TP).wait_recv()
+    with jax.named_scope('o_on_1'):
+        output_on(1, begin)
+    with jax.named_scope('share'):
+        share(begin)
+    with jax.named_scope('o_on_2'):
+        output_on(2, begin)
+    with jax.named_scope('share_aside'):
+        share_aside(begin)
+    for d in range(3, Z):
+        with jax.named_scope('o_on_3'):
+            output_on(d, begin)
+    with jax.named_scope('share_wait'):
+        for k in range(1, Z):
+            l_across(k, back_z(k)).wait_recv()
+        for k in range(XH):
+            for zz in range(Z):
+                j_twin(zz, k, (twin + TP - 2 * k) % TP).wait_recv()
 
     mem_base = TP * sinks.shape[0] * HD
     per_tp = sinks.shape[0] * HD
     half = N // 2
-    LTF[...] = jnp.zeros_like(LTF)
     for zz in range(Z):
         for t in range(TP):
             at = t * per_tp + zz * LANES
@@ -506,14 +608,14 @@
             at = mem_base + (t * Z + zz) * HD
             X[:half, at : at + HD] = J[t, zz, N:, :HD]
             X[half:, at : at + HD] = J[t, zz, N:, HD:]
-        LTF[2 * zz : 2 * zz + 2, :] = LT[zz, 0:2, :]
-    totals[...] = LTF[...].T[:, : sinks.shape[0]]
-
-    keep[2].wait()
-    for zz in range(Z):
-        for k in range(1, Y):
-            for c in range(OC):
-                o_side(zz, k, c, back_y(k), False).wait_recv()
+        totals[2 * zz : 2 * zz + 2, :] = LT[zz, 0:2, :]
+
+    with jax.named_scope('o_wait'):
+        keep[8].wait()
+        for zz in range(Z):
+            for k in range(1, Y):
+                for c in range(OC):
+                    o_side(zz, k, c, back_y(k), False).wait_recv()
 
     tile = 256
 
@@ -522,14 +624,20 @@
         mixed[:, cols] = dot(X[...], O[:, cols]).astype(jnp.bfloat16)
         return nothing
 
-    lax.fori_loop(0, mixed.shape[1] // tile, columns, 0)
-
-    weights_out(drain)
+    with jax.named_scope('out_matmul'):
+        lax.fori_loop(0, mixed.shape[1] // tile, columns, 0)
+
     own_tokens(drain)
-    weights_on(drain)
+    weights_far(drain)
+    weights_aside(z, drain)
+    output_aside(drain)
     own_output(drain)
+    for k in range(1, Z):
+        f_across(k, z).wait_send()
 
     def settle(i, nothing):
+        near(i, drain)
+        weights_on(i, drain)
         tokens_on(i, drain)
         output_on(i, drain)
         return nothing
@@ -542,16 +650,19 @@
             s_side(zz, k, y).wait_send()
     hand_over(drain)
     share(drain)
-
-
-def mix(tokens, gain, packed, shifts, gate_cols, w_out, sinks, bias):
+    share_aside(drain)
+
+
+def mix(tokens, gain, shifts, gates, w_out, weights, sinks, bias):
     S, TP = lax.axis_size("sp"), lax.axis_size("tp")
-    Z = packed.shape[0]
+    Z = shifts.shape[0]
     Y, XH = S // Z, TP // 2
     R, D = tokens.shape
     N = R * TP
-    C = packed.shape[2]
+    KD = weights[0].shape[0]
+    C = sum(part.shape[1] for part in weights[3:]) // Z + weights[0].shape[1] // Z + 2 * HD
     TC = OC = 3
+    WC = 2
     M = w_out.shape[1]
     bf, f32 = jnp.bfloat16, jnp.float32
     dma = pltpu.SemaphoreType.DMA
@@ -560,33 +671,37 @@
     smem = pl.BlockSpec(memory_space=pltpu.SMEM)
     hbm = pl.BlockSpec(memory_space=pl.ANY)
     return pl.pallas_call(
-        functools.partial(mixer_kernel, (Z, Y, TP, TC, OC)),
+        functools.partial(mixer_kernel, (Z, Y, TP, TC, WC, OC)),
         out_shape=[
             jax.ShapeDtypeStruct((N, M), bf),
-            jax.ShapeDtypeStruct((N, sinks.shape[0]), f32),
+            jax.ShapeDtypeStruct((sinks.shape[0], N), f32),
         ],
-        in_specs=[vmem, vmem, hbm, vmem, hbm, hbm, smem, smem],
+        in_specs=[vmem] * 3 + [hbm] * 9 + [smem] * 2,
         out_specs=[vmem, vmem],
-        scratch_shapes=[
+        scratch_shapes=[pltpu.VMEM(part.shape, bf) for part in weights]
+        + [
+            pltpu.VMEM((Z, KD, C), bf),
             pltpu.VMEM((Z * N, D), bf),
             pltpu.VMEM((D, C), bf),
-            pltpu.VMEM((D, LANES), bf),
+            pltpu.VMEM(gates.shape, bf),
             pltpu.VMEM((S * w_out.shape[0], M), bf),
-            pltpu.VMEM((N, C + LANES), f32),
+            pltpu.VMEM((Z * N, C + LANES), f32),
+            pltpu.VMEM((LANES, N), f32),
             pltpu.VMEM((Z * N, C), bf),
             pltpu.VMEM((Z * N, LANES), f32),
             pltpu.VMEM((S, HD, LANES), f32),
             pltpu.VMEM((Z, HD, LANES), f32),
             pltpu.VMEM((Z + 1, WINDOW, LANES), bf),
             pltpu.VMEM((Z, 8, N), f32),
+            pltpu.VMEM((Z, 8, N), f32),
             pltpu.VMEM((Z, piece, LANES), bf),
             pltpu.VMEM((TP, Z, piece, LANES), bf),
             pltpu.VMEM((Z, 8, N), f32),
             pltpu.VMEM((Z, 8, N), f32),
-            pltpu.VMEM((LANES, N), f32),
             pltpu.VMEM((N, S * w_out.shape[0]), bf),
-            dma((3,)),
-            dma((Z,)), dma((Z,)), dma((Z, Y - 1)), dma((Z, Y - 1)), dma((Z,)), dma((Z,)),
+            dma((9,)),
+            dma((2, Z, WC)), dma((2, Z, WC)), dma((Y - 1, Z, WC)), dma((Y - 1, Z, WC)),
+            dma((Z,)), dma((Z,)),
             dma((2, Z, TC)), dma((Z, TC)), dma((XH - 1, Z, TC)), dma((XH - 1, Z, TC)),
             dma((XH, Z, TC)), dma((XH, Z, TC)),
             dma((2, Z, OC)), dma((Z, OC)), dma((Y - 1, Z, OC)), dma((Y - 1, Z, OC)),
@@ -597,7 +712,7 @@
         compiler_params=pltpu.CompilerParams(
             collective_id=0, has_side_effects=True, vmem_limit_bytes=60 * 2**20
         ),
-    )(tokens, gain, packed, shifts, gate_cols, w_out, sinks, bias)
+    )(tokens, gain, shifts, gates, w_out, *weights, sinks, bias)
 
 
 def shards(
@@ -616,36 +731,18 @@
     forget_shift,
     w_out,
 ):
-    mem_heads = forget_bias.shape[0]
-    Z = mem_heads
-    Y = lax.axis_size("sp") // Z
-    z, tp = lax.axis_index("sp") // Y, lax.axis_index("tp")
-    q_width = w_query.shape[1] // Z
-    per_z = q_width // HD
-    group = w_query.shape[1] // w_key.shape[1]
-
-    def piece(i):
-        kv = i * per_z // group * HD
-        mem = [
-            part[:, i * HD : (i + 1) * HD]
-            for part in (w_mem_query, w_mem_key, w_mem_value, w_mem_gate)
-        ]
-        return jnp.concatenate(
-            [w_query[:, i * q_width : (i + 1) * q_width]]
-            + mem
-            + [w_key[:, kv : kv + HD], w_value[:, kv : kv + HD]],
-            axis=1,
-        )
-
-    packed = jnp.stack([piece(i) for i in range(Z)])
-    head = tp * mem_heads + z
-    gate_cols = lax.dynamic_slice_in_dim(w_gates, head, 1, 2)[:, :, 0]
-    gate_cols = jnp.pad(gate_cols, ((0, 0), (0, LANES - 2)))
-    shifts = jnp.pad(forget_shift.T[:, None, :], ((0, 0), (0, 7), (0, 0)))
+    weights = (w_query, w_key, w_value, w_mem_query, w_mem_key, w_mem_value, w_mem_gate)
     mixed, totals = mix(
-        tokens, norm_gain[None, :], packed, shifts, gate_cols, w_out, sinks, forget_bias
+        tokens,
+        norm_gain[None, :],
+        forget_shift.T,
+        w_gates.reshape(w_gates.shape[0], -1),
+        w_out,
+        weights,
+        sinks,
+        forget_bias,
     )
-    return mixed, totals
+    return mixed, totals.T
 
 
 def solution(mesh):

time: 228 us -> 197 us (0.86)
  Pallas kernels: 210 us -> 191 us
  local copies, waits for them, and re-layouts: 13.4 us -> 4.94 us
    pallas_call x1, Pallas kernels: 210 us -> 191 us  [mix(): pl.pallas_call(functools.partial(mixer_kernel, (Z, Y, TP, TC, WC, OC)), o...]
    concatenate x4 -> x0, local copies, waits for them, and re-layouts: 3.94 us -> none  [piece(): jnp.concatenate([w_query[:, i * q_width:(i + 1) * q_width]] + mem + [w_ke...]
    slice x4 -> x0, local copies, waits for them, and re-layouts: 2.74 us -> none  [the longest x2 1.82 us: piece(): part[:, i * HD:(i + 1) * HD]]
where the time goes in v1:
time: 197 us
  Pallas kernels  191 us (97%)
  local copies, waits for them, and re-layouts  4.94 us (3%)
    pallas_call x1, Pallas kernels, mix(): pl.pallas_call(functools.partial(mixer_kernel, (Z, Y, TP, TC, WC, OC)), o...  191 us

profile of v1, /device:TPU:0, one launch (start us, length us, event | category | flops | bytes accessed | tf_op | source)
XLA Modules:
  0.0 196.8 jit_solution(7455661901623830244)
XLA Ops:
  0.6 2.3 %copy.17.gates = bf16[4096,32]{1,0:T(8,128)(2,1)} copy(bf16[4096,32]{0,1:T(8,128)(2,1)} %bitcast.4) | data formatting | bytes 524288 | tf_op jit(solution)/shard_map/reshape | solution.py:739
  2.9 191.2 %shard_map.149 = (bf16[384,1024]{1,0:T(8,128)(2,1)}, f32[8,384]{1,0:T(8,128)}) custom-call(bf16[96,4096]{1,0:T(8,128)(2,1)} %tokens.1, f32[1,4096]{1,0:T(1,128)} %bitcast.5, f32[4,384]{1,0:T(4,128)} %bitcast.7, bf16[4096,32]{1,0:T(8,128)(2,1)} %copy.17.gates, bf16[384,1024]{1,0:T(8,128)(2,1)} %w_out.1, bf16[512,512]{1,0:T(8,128)(2,1)} %w_query.1, ...), custom_call_target="tpu_custom_call" | custom-call | tf_op jit(solution)/shard_map/pallas_call | solution.py:673
  194.1 0.0 copy-start
  194.1 2.1 %copy.20 = bf16[384,1024]{1,0:T(8,128)(2,1)} copy(bf16[384,1024]{1,0:T(8,128)(2,1)} %get-tuple-element.8) | data formatting | bytes 1572864
  196.2 0.0 copy-done
  196.2 0.6 copy.21
Async XLA Ops:
  194.1 2.1 %copy-start = (f32[8,384]{1,0:T(8,128)S(1)}, f32[8,384]{1,0:T(8,128)}, u32[]{:S(2)}) copy-start(f32[8,384]{1,0:T(8,128)} %get-tuple-element.5) | copy-start | bytes 36868

commit v2 on v1

--- a/solution.py
+++ b/solution.py
@@ -38,24 +38,33 @@
     w_mem_value, w_mem_gate, sinks, bias,
     mixed, totals,
     in_query, in_key, in_value, in_mem_query, in_mem_key, in_mem_value, in_mem_gate,
-    PACK, T, W, GW, O, ACC, FLAT, PROJ, NUM, ST, EB, HALO, SH, FS, JS, J, LS, LT, X,
-    own_sems, w_send, w_recv, wy_send, wy_recv, f_send, f_recv,
-    tz_send, tz_recv, tx_send, tx_recv, tt_send, tt_recv,
-    oz_send, oz_recv, oy_send, oy_recv,
-    h_send, h_recv, s_send, s_recv,
-    jz_send, jz_recv, l_send, l_recv, jx_send, jx_recv, jt_send, jt_recv,
+    PM, PA, T, WM, WA, GW, O, ACC, ACCA, FLAT, PROJ, PROJA, NUM, ST, EB, HALO, SH, FS,
+    JSM, JSA, JM, JA, LS, LT, X, MIX,
+    own_sems, w_send, w_recv, wa_send, wa_recv, wy_send, wy_recv, wb_send, wb_recv,
+    f_send, f_recv, tz_send, tz_recv, tx_send, tx_recv, tt_send, tt_recv,
+    oz_send, oz_recv, oy_send, oy_recv, h_send, h_recv, s_send, s_recv,
+    jz_send, jz_recv, ja_send, ja_recv, l_send, l_recv,
+    jx_send, jx_recv, jt_send, jt_recv, jxa_send, jxa_recv, jta_send, jta_recv,
 ):
     Z, Y, TP, TC, WC, OC = sizes
     XH = TP // 2
     R, D = tokens.shape
     N = R * TP
-    KD, C = PACK.shape[1:]
-    KO = w_out.shape[0]
-    RC, RW, RO = R // TC, KD // WC, KO // OC
+    HOLD, KD, CA = PA.shape
+    CM = PM.shape[2]
+    offset = (Z - HOLD) // 2
+    KO, M = w_out.shape
+    MC = WC // 2
+    RC, RW, RM, RO = R // TC, KD // WC, KD // MC, KO // OC
     S = Z * Y
     sp, tp = lax.axis_index("sp"), lax.axis_index("tp")
     z, y = sp // Y, sp % Y
     twin = tp + 1 - 2 * (tp % 2)
+
+    def is_holder(zz):
+        return (zz >= offset) & (zz < offset + HOLD)
+
+    holds = is_holder(z)
     can_up, can_down = z < Z - 1, z > 0
 
     def remote(src, dst, send, recv, to_sp, to_tp):
@@ -82,27 +91,36 @@
     def back_y(k):
         return (y + Y - k) % Y
 
-    def w_rows(zz, yy, c):
-        return W.at[pl.ds(pl.multiple_of((zz * Y + yy) * KD + c * RW, RW), RW), :]
-
-    def w_across(way, d, c):
+    def m_rows(zz, yy, c):
+        return WM.at[pl.ds(pl.multiple_of((zz * Y + yy) * KD + c * RM, RM), RM), :]
+
+    def a_rows(zz, yy, c):
+        return WA.at[pl.ds(pl.multiple_of((zz * Y + yy) * KD + c * RW, RW), RW), :]
+
+    def m_across(way, d, c, source, piece):
         to = z + d * (1 - 2 * way)
         return remote(
-            PACK.at[to, pl.ds(c * RW, RW), :], w_rows(z, y, c),
+            PM.at[piece, pl.ds(c * RM, RM), :], m_rows(source, y, c),
             w_send.at[way, d, c], w_recv.at[way, d, c], to * Y + y, tp,
         )
 
-    def w_landed(way, d, c):
-        origin = z - d * (1 - 2 * way)
+    def a_across(way, d, c, source, piece):
+        to = z + d * (1 - 2 * way)
         return remote(
-            PACK.at[z, pl.ds(c * RW, RW), :], w_rows(origin, y, c),
-            w_send.at[way, d, c], w_recv.at[way, d, c], sp, tp,
-        )
-
-    def w_side(zz, j, c, source):
-        place = w_rows(zz, source, c)
+            PA.at[piece, pl.ds(c * RW, RW), :], a_rows(source, y, c),
+            wa_send.at[way, d, c], wa_recv.at[way, d, c], to * Y + y, tp,
+        )
+
+    def m_side(zz, j, c, source):
+        place = m_rows(zz, source, c)
         return remote(
             place, place, wy_send.at[j - 1, zz, c], wy_recv.at[j - 1, zz, c], z * Y + up_y(j), tp
+        )
+
+    def a_side(zz, j, c, source):
+        place = a_rows(zz, source, c)
+        return remote(
+            place, place, wb_send.at[j - 1, zz, c], wb_recv.at[j - 1, zz, c], z * Y + up_y(j), tp
         )
 
     def f_across(k, source):
@@ -145,7 +163,7 @@
     def h_side(zz, shift):
         rows = pl.ds(pl.multiple_of(zz * N + N - WINDOW, WINDOW), WINDOW)
         return remote(
-            PROJ.at[rows, pl.ds(3 * LANES, LANES)], HALO.at[zz + shift],
+            PROJA.at[rows, pl.ds(CA - LANES, LANES)], HALO.at[zz + shift],
             h_send.at[zz], h_recv.at[zz], z * Y + up_y(1), tp,
         )
 
@@ -154,23 +172,40 @@
         return remote(place, place, s_send.at[k - 1, zz], s_recv.at[k - 1, zz], z * Y + up_y(k), tp)
 
     def j_across(k, source):
-        return remote(JS.at[up_z(k)], J.at[tp, source], jz_send.at[k], jz_recv.at[k], up_z(k) * Y + y, tp)
-
-    def l_across(k, source):
-        return remote(LS.at[up_z(k)], LT.at[source], l_send.at[k], l_recv.at[k], up_z(k) * Y + y, tp)
+        return remote(
+            JSM.at[up_z(k)], JM.at[tp, source], jz_send.at[k], jz_recv.at[k], up_z(k) * Y + y, tp
+        )
+
+    def ja_across(k, holder):
+        return remote(
+            JSA.at[up_z(k)], JA.at[tp, holder], ja_send.at[k], ja_recv.at[k], up_z(k) * Y + y, tp
+        )
+
+    def l_across(k, holder):
+        return remote(
+            LS.at[up_z(k)], LT.at[holder], l_send.at[k], l_recv.at[k], up_z(k) * Y + y, tp
+        )
 
     def j_side(zz, k, source):
-        place = J.at[source, zz]
+        place = JM.at[source, zz]
         return remote(place, place, jx_send.at[k - 1, zz], jx_recv.at[k - 1, zz], sp, side_tp(k))
 
     def j_twin(zz, k, source):
-        place = J.at[source, zz]
+        place = JM.at[source, zz]
         return remote(place, place, jt_send.at[k, zz], jt_recv.at[k, zz], sp, twin)
+
+    def ja_side(a, k, source):
+        place = JA.at[source, a]
+        return remote(place, place, jxa_send.at[k - 1, a], jxa_recv.at[k - 1, a], sp, side_tp(k))
+
+    def ja_twin(a, k, source):
+        place = JA.at[source, a]
+        return remote(place, place, jta_send.at[k, a], jta_recv.at[k, a], sp, twin)
 
     ins = (
         (w_query, in_query), (w_key, in_key), (w_value, in_value), (w_mem_query, in_mem_query),
         (w_mem_key, in_mem_key), (w_mem_value, in_mem_value), (w_mem_gate, in_mem_gate),
-        (gates, GW), (w_out, O.at[pl.ds(pl.multiple_of(sp * KO, KO), KO), :]),
+        (w_out, O.at[pl.ds(pl.multiple_of(sp * KO, KO), KO), :]),
     )
     keep = [pltpu.make_async_copy(a, b, own_sems.at[i]) for i, (a, b) in enumerate(ins)]
 
@@ -205,9 +240,9 @@
     def pack():
         for copy in keep[:7]:
             copy.wait()
-        group = w_query.shape[1] // w_key.shape[1]
         high = min(KD, WINDOW)
         lane = lanes_of((high, LANES))
+        qa = CA - LANES
 
         def halves(rows, left, i, right, j):
             a = left[rows, pl.ds(i // 2 * LANES, LANES)].astype(jnp.float32)
@@ -219,48 +254,70 @@
         def some(r, nothing):
             rows = pl.ds(pl.multiple_of(r * high, high), high)
             for i in range(Z):
-                kv = i * (LANES // HD) // group
-                PACK[i, rows, :LANES] = in_query[rows, i * LANES : (i + 1) * LANES]
-                for n, parts in enumerate(
-                    (
-                        (in_mem_query, i, in_mem_key, i),
-                        (in_mem_value, i, in_mem_gate, i),
-                        (in_key, kv, in_value, kv),
-                    )
-                ):
-                    PACK[i, rows, (n + 1) * LANES : (n + 2) * LANES] = halves(rows, *parts)
+                PM[i, rows, :LANES] = halves(rows, in_mem_query, i, in_mem_key, i)
+                PM[i, rows, LANES:] = halves(rows, in_mem_value, i, in_mem_gate, i)
+            for i in range(HOLD):
+                PA[i, rows, :qa] = in_query[rows, i * qa : (i + 1) * qa]
+                PA[i, rows, qa:] = halves(rows, in_key, i, in_value, i)
             return nothing
 
         lax.fori_loop(0, KD // high, some, 0)
-        W[pl.ds(pl.multiple_of(sp * KD, KD), KD), :] = PACK[z]
+        rows = pl.ds(pl.multiple_of(sp * KD, KD), KD)
+        WM[rows, :] = PM[z]
+
+        @pl.when(holds)
+        def _():
+            WA[rows, :] = PA[z - offset]
 
     def ways(d):
         return ((0, z + d < Z, z - d >= 0), (1, z - d >= 0, z + d < Z))
 
     def weights_out(way, d, act):
-        for c in range(WC):
-            act(w_across(way, d, c))
+        to = z + d * (1 - 2 * way)
+
+        @pl.when(is_holder(to))
+        def _():
+            for c in range(WC):
+                act(a_across(way, d, c, z, to - offset))
+
+        for c in range(MC):
+            act(m_across(way, d, c, z, to))
 
     def weights_far(act):
-        for d in range(2, Z):
+        for d in range(Z - 1, 1, -1):
             for way, there, _ in ways(d):
                 pl.when(there)(lambda: weights_out(way, d, act))
 
     def weights_aside(zz, act):
-        for c in range(WC):
-            for j in range(1, Y):
-                act(w_side(zz, j, c, y))
+        for j in range(1, Y):
+            for c in range(MC):
+                act(m_side(zz, j, c, y))
+
+            @pl.when(holds)
+            def _():
+                for c in range(WC):
+                    act(a_side(zz, j, c, y))
 
     def weights_on(d, act):
         for way, _, there in ways(d):
-            def landed(way=way):
+            origin = z - d * (1 - 2 * way)
+
+            def landed_a(way=way, origin=origin):
                 for c in range(WC):
                     if act is begin:
-                        w_landed(way, d, c).wait_recv()
+                        a_across(way, d, c, origin, 0).wait_recv()
                     for j in range(1, Y):
-                        act(w_side(z - d * (1 - 2 * way), j, c, y))
-
-            pl.when(there)(landed)
+                        act(a_side(origin, j, c, y))
+
+            def landed_m(way=way, origin=origin):
+                for c in range(MC):
+                    if act is begin:
+                        m_across(way, d, c, origin, 0).wait_recv()
+                    for j in range(1, Y):
+                        act(m_side(origin, j, c, y))
+
+            pl.when(there & holds)(landed_a)
+            pl.when(there)(landed_m)
 
     def own_tokens(act):
         for c in range(TC):
@@ -302,19 +359,30 @@
             pl.when(can_up)(lambda: act(o_line(z, 0, c, True)))
             pl.when(can_down)(lambda: act(o_line(z, 1, c, True)))
 
-    def output_on(d, act):
+    def output_on(d, act, line=True, aside=True):
         for way, origin, there, further in (
             (0, z - d, z - d >= 0, can_up), (1, z + d, z + d < Z, can_down),
         ):
             def landed(way=way, origin=origin, further=further):
                 for c in range(OC):
-                    if act is begin:
+                    if act is begin and line:
                         o_line(origin, way, c, False).wait_recv()
-                    pl.when(further)(lambda: act(o_line(origin, way, c, False)))
-                    for k in range(1, Y):
-                        act(o_side(origin, k, c, y, False))
+                    if line:
+                        pl.when(further)(lambda: act(o_line(origin, way, c, False)))
+                    if aside:
+                        for k in range(1, Y):
+                            act(o_side(origin, k, c, y, False))
 
             pl.when(there)(landed)
+
+    def output_pieces(first, last, act):
+        for c, way in [(c, way) for c in range(OC) for way in range(2)][first:last]:
+            origin = z - 1 + 2 * way
+
+            @pl.when((origin >= 0) & (origin < Z))
+            def _():
+                for k in range(1, Y):
+                    act(o_side(origin, k, c, y, False))
 
     def block_rows(zz):
         return pl.ds(pl.multiple_of(zz * N, N), N)
@@ -327,8 +395,13 @@
         def part(b, nothing):
             rows = block_rows(b)
             block = T[rows, cols]
-            ACC[rows, :C] += dot(block, W[cols, :])
-            ACC[rows, C : C + GW.shape[1]] += dot(block, GW[cols, :])
+            ACC[rows, :CM] += dot(block, WM[cols, :])
+            ACC[rows, CM:] += dot(block, GW[cols, :])
+
+            @pl.when(holds)
+            def _():
+                ACCA[rows, :] += dot(block, WA[cols, :])
+
             return nothing
 
         lax.fori_loop(0, Z, part, 0)
@@ -339,13 +412,13 @@
     def sub_rows(zz, i):
         return pl.ds(pl.multiple_of(zz * N + i * WINDOW, WINDOW), WINDOW)
 
-    def attend(zz, i, before):
+    def attend(zz, i, before, pair):
         lane = lanes_of(wide)
-        heads = PROJ[sub_rows(zz, i), :LANES].astype(jnp.float32) * HD ** (-0.5)
+        heads = PROJA[sub_rows(zz, i), pair * LANES : (pair + 1) * LANES].astype(jnp.float32) * HD ** (-0.5)
         first = jnp.where(lane < HD, heads, 0.0)
         second = jnp.where(lane < HD, pltpu.roll(heads, HD, 1), 0.0)
         query = jnp.concatenate([first, second], axis=0).astype(jnp.bfloat16)
-        rows = jnp.concatenate([before, PROJ[sub_rows(zz, i), 3 * LANES :]], axis=0)
+        rows = jnp.concatenate([before, PROJA[sub_rows(zz, i), CA - LANES :]], axis=0)
         scores = lax.dot_general(
             query, rows, (((1,), (1,)), ((), ())), preferred_element_type=jnp.float32
         )
@@ -360,21 +433,22 @@
             allowed = allowed & (key_at >= lowest)
         scores = jnp.where(allowed, scores, MASKED)
         tall = lax.broadcasted_iota(jnp.int32, (2 * WINDOW, 1), 0) >= WINDOW
-        sink = jnp.where(tall, sinks[2 * z + 1], sinks[2 * z])
+        at_sink = (z - offset) * (CA - LANES) // HD + 2 * pair
+        sink = jnp.where(tall, sinks[at_sink + 1], sinks[at_sink])
         ceiling = jnp.maximum(jnp.max(scores, axis=-1, keepdims=True), sink)
         weights = jnp.exp(scores - ceiling)
         total = jnp.exp(sink - ceiling) + jnp.sum(weights, axis=-1, keepdims=True)
         probs = (weights * (1.0 / total)).astype(jnp.bfloat16)
         out = dot(probs, rows)
         both = jnp.where(lane < HD, pltpu.roll(out[:WINDOW], HD, 1), out[WINDOW:])
-        JS[zz, pl.ds(i * WINDOW, WINDOW), :] = both.astype(jnp.bfloat16)
+        JSA[zz, pl.ds(pair * N + i * WINDOW, WINDOW), :] = both.astype(jnp.bfloat16)
         logs = jnp.broadcast_to(ceiling + jnp.log(total), (2 * WINDOW, LANES)).T
-        LS[zz, 0:1, pl.ds(i * WINDOW, WINDOW)] = logs[0:1, :WINDOW]
-        LS[zz, 1:2, pl.ds(i * WINDOW, WINDOW)] = logs[0:1, WINDOW:]
+        LS[zz, 2 * pair : 2 * pair + 1, pl.ds(i * WINDOW, WINDOW)] = logs[0:1, :WINDOW]
+        LS[zz, 2 * pair + 1 : 2 * pair + 2, pl.ds(i * WINDOW, WINDOW)] = logs[0:1, WINDOW:]
 
     def remember(zz):
-        FLAT[...] = ACC[block_rows(zz), C:].T
-        gate_count = GW.shape[1] // 2
+        FLAT[...] = ACC[block_rows(zz), CM:].T
+        gate_count = gates.shape[0] // 2
         head = tp * Z + z
         log_in = FLAT[pl.ds(head, 1), :] - 0.5 * math.log(N * S)
         pre = FLAT[pl.ds(gate_count + head, 1), :] + bias[z]
@@ -392,11 +466,11 @@
         decays = passed - summed + log_in
         level = jnp.max(decays, axis=1, keepdims=True)
         weights = jnp.exp(decays - level)
-        pair = PROJ[block_rows(zz), LANES : 2 * LANES].astype(jnp.float32)
+        pair = PROJ[block_rows(zz), :LANES].astype(jnp.float32)
         query = (pair[:, :HD] * HD ** (-0.5)).astype(jnp.bfloat16)
         keys = pair.T[HD:, :]
         lane = lanes_of((N, LANES))
-        values = PROJ[block_rows(zz), 2 * LANES : 3 * LANES].astype(jnp.float32)
+        values = PROJ[block_rows(zz), LANES:].astype(jnp.float32)
         values = jnp.where(lane < HD, values, jnp.where(lane == HD, 1.0, 0.0)).astype(jnp.bfloat16)
         state = dot((keys * weights).astype(jnp.bfloat16), values)
         lane = lanes_of(state.shape)
@@ -424,15 +498,30 @@
             )
 
     def local_work(zz):
-        PROJ[block_rows(zz), :] = ACC[block_rows(zz), :C].astype(jnp.bfloat16)
+        PROJ[block_rows(zz), :] = ACC[block_rows(zz), :CM].astype(jnp.bfloat16)
+
+        @pl.when(holds)
+        def _():
+            PROJA[block_rows(zz), :] = ACCA[block_rows(zz), :].astype(jnp.bfloat16)
+
         with jax.named_scope('remember'):
             remember(zz)
-        h_side(zz, (y + 1) // Y).start()
-        with jax.named_scope('attend'):
-            for i in range(1, parts):
-                attend(zz, i, PROJ[sub_rows(zz, i - 1), 3 * LANES :])
+
+        @pl.when(holds)
+        def _():
+            h_side(zz, (y + 1) // Y).start()
+            with jax.named_scope('attend'):
+                for i in range(1, parts):
+                    before = PROJA[sub_rows(zz, i - 1), CA - LANES :]
+                    for pair in range(CA // LANES - 1):
+                        attend(zz, i, before, pair)
+
         for k in range(1, Y):
             s_side(zz, k, y).start()
+
+    def near(d, act):
+        pl.when((z == d) & can_up)(lambda: weights_out(0, 1, act))
+        pl.when((z == Z - 1 - d) & can_down)(lambda: weights_out(1, 1, act))
 
     own_tokens(begin)
     with jax.named_scope('pack'):
@@ -441,7 +530,21 @@
         f_across(k, z).start()
     weights_aside(z, begin)
     output_aside(begin)
+    near(0, begin)
     ACC[...] = jnp.zeros_like(ACC)
+    ACCA[...] = jnp.zeros_like(ACCA)
+
+    def turn(i, nothing):
+        cols = pl.ds(pl.multiple_of(i * LANES, LANES), LANES)
+        count = gates.shape[0]
+        tall = jnp.concatenate(
+            [gates[:, cols].astype(jnp.float32), jnp.zeros((LANES - count, LANES), jnp.float32)],
+            axis=0,
+        )
+        GW[cols, :] = tall.T.astype(jnp.bfloat16)
+        return nothing
+
+    lax.fori_loop(0, D // LANES, turn, 0)
 
     def both_sides(d, act):
         def one(side, nothing):
@@ -451,61 +554,90 @@
 
         lax.fori_loop(0, 2, one, 0)
 
-    def near(d, act):
-        pl.when((z == d - 1) & can_up)(lambda: weights_out(0, 1, act))
-        pl.when((z == Z - d) & can_down)(lambda: weights_out(1, 1, act))
-
     def stage(d, nothing):
-        near(d, begin)
         with jax.named_scope('t_on'):
             tokens_on(d, begin)
+        near(d, begin)
+
+        inside = can_up & can_down
+
+        @pl.when((d == Z - 1) & jnp.logical_not(inside))
+        def _():
+            weights_far(begin)
+
+        @pl.when((d == Z - 1) & inside)
+        def _():
+            weights_far(begin)
+
+        pl.when(d == Z - 1)(lambda: own_output(begin))
+
+        @pl.when((d == 2) & inside)
+        def _():
+            with jax.named_scope('w_on_mid'):
+                weights_on(1, begin)
+
         with jax.named_scope('t_aside'):
             both_sides(d - 1, lambda zz: tokens_aside(zz, begin))
         return nothing
 
     lax.fori_loop(1, Z, stage, 0)
-    weights_far(begin)
-    own_output(begin)
-    with jax.named_scope('w_on_1'):
-        weights_on(1, begin)
+    with jax.named_scope('w_on_3'):
+        for d in range(Z - 1, 2, -1):
+            weights_on(d, begin)
     with jax.named_scope('t_last'):
         both_sides(Z - 1, lambda zz: tokens_aside(zz, begin))
         for zz in range(Z):
             for k in range(XH):
                 for c in range(TC):
                     t_twin(zz, k, c, (twin + TP - 2 * k) % TP).wait_recv()
-    keep[7].wait()
 
     def multiply(zz):
         with jax.named_scope('w_side'):
             for j in range(1, Y):
-                for c in range(WC):
-                    w_side(zz, j, c, back_y(j)).wait_recv()
+                for c in range(MC):
+                    m_side(zz, j, c, back_y(j)).wait_recv()
+
+                @pl.when(holds)
+                def _():
+                    for c in range(WC):
+                        a_side(zz, j, c, back_y(j)).wait_recv()
+
         with jax.named_scope('project'):
             project(zz)
 
-    def stage_two(d, nothing):
-        @pl.when((d > 0) & (d + 1 < Z))
-        def _():
-            with jax.named_scope('w_on'):
-                weights_on(d + 1, begin)
-
+    both_sides(0, multiply)
+
+    @pl.when(jnp.logical_not(can_up & can_down))
+    def _():
+        with jax.named_scope('w_on_1'):
+            weights_on(1, begin)
+
+    for d in range(Z - 1, 2, -1):
         both_sides(d, multiply)
-        return nothing
-
-    lax.fori_loop(0, Z, stage_two, 0)
+    if Z > 2:
+        with jax.named_scope('w_on_2'):
+            weights_on(2, begin)
+    for d in range(1, min(Z, 3)):
+        both_sides(d, multiply)
     for k in range(1, Z):
         f_across(k, back_z(k)).wait_recv()
 
+    with jax.named_scope('o_line_1'):
+        output_on(1, begin, aside=False)
+
     def local(zz, nothing):
         local_work(zz)
+        for i in range(4):
+            pl.when(zz == i)(lambda: output_pieces(i, 1 + i, begin))
         return nothing
 
     lax.fori_loop(0, Z, local, 0)
+
+    output_pieces(4, 2 * OC, begin)
 
     with jax.named_scope('halo_state'):
         for zz in range(Z):
-            h_side(zz, 1 - jnp.minimum(y, 1)).wait_recv()
+            pl.when(holds)(lambda: h_side(zz, 1 - jnp.minimum(y, 1)).wait_recv())
             for k in range(1, Y):
                 s_side(zz, k, back_y(k)).wait_recv()
 
@@ -527,12 +659,16 @@
     enter()
 
     def finish(zz):
-        attend(zz, 0, HALO[zz])
+        @pl.when(holds)
+        def _():
+            for pair in range(CA // LANES - 1):
+                attend(zz, 0, HALO[zz], pair)
+
         entering = EB[zz]
         stabilizer = entering[0:1, HD + 1 : HD + 2]
         local = NUM[block_rows(zz), :]
         peak, since = local[:, HD + 1 : HD + 2], local[:, HD + 2 : HD + 3]
-        pair = PROJ[block_rows(zz), LANES : 2 * LANES].astype(jnp.float32)
+        pair = PROJ[block_rows(zz), :LANES].astype(jnp.float32)
         query = (pair[:, :HD] * HD ** (-0.5)).astype(jnp.bfloat16)
         carried = dot(query, entering.astype(jnp.bfloat16))
         older = since + stabilizer
@@ -540,92 +676,125 @@
         found = jnp.exp(older - row_level) * carried + jnp.exp(peak - row_level) * local
         bound = jnp.maximum(jnp.abs(found[:, HD : HD + 1]), jnp.exp(-row_level))
         gate = pltpu.roll(
-            PROJ[block_rows(zz), 2 * LANES : 3 * LANES].astype(jnp.float32), HD, 1
+            PROJ[block_rows(zz), LANES:].astype(jnp.float32), HD, 1
         )
         recall = found / bound * jax.nn.sigmoid(gate)
         half = N // 2
         lane = lanes_of((half, LANES))
         paired = jnp.where(lane < HD, recall[:half], pltpu.roll(recall[half:], HD, 1))
-        JS[zz, N:, :] = paired.astype(jnp.bfloat16)
-
-    def hand_over(act):
-        for k in range(1, Z):
-            act(j_across(k, z))
-            act(l_across(k, z))
+        JSM[zz] = paired.astype(jnp.bfloat16)
+
+    def hand_over(k, act):
+        act(j_across(k, z))
+
+        @pl.when(holds)
+        def _():
+            act(ja_across(k, z - offset))
+            act(l_across(k, z - offset))
 
     for k in range(1, Z):
         with jax.named_scope('finish'):
             finish(up_z(k))
-        j_across(k, z).start()
-        l_across(k, z).start()
+        hand_over(k, begin)
     with jax.named_scope('finish'):
         finish(z)
-    J[tp, z] = JS[z]
-    LT[z] = LS[z]
-
-    def share(act):
-        for k in range(Z):
-            zz = back_z(k)
+    JM[tp, z] = JSM[z]
+
+    @pl.when(holds)
+    def _():
+        JA[tp, z - offset] = JSA[z]
+        LT[z - offset] = LS[z]
+
+    def share(k, act):
+        zz = back_z(k)
+        if k and act is begin:
+            j_across(k, zz).wait_recv()
+        for j in range(1, XH):
+            act(j_side(zz, j, tp))
+        act(j_twin(zz, 0, tp))
+
+        @pl.when(is_holder(zz))
+        def _():
             if k and act is begin:
-                j_across(k, zz).wait_recv()
+                ja_across(k, zz - offset).wait_recv()
             for j in range(1, XH):
-                act(j_side(zz, j, tp))
-            act(j_twin(zz, 0, tp))
+                act(ja_side(zz - offset, j, tp))
+            act(ja_twin(zz - offset, 0, tp))
 
     def share_aside(act):
-        for k in range(Z):
-            zz = back_z(k)
+        for zz in range(Z):
             for j in range(1, XH):
                 if act is begin:
                     j_side(zz, j, from_tp(j)).wait_recv()
                 act(j_twin(zz, j, from_tp(j)))
-
-    with jax.named_scope('o_on_1'):
-        output_on(1, begin)
-    with jax.named_scope('share'):
-        share(begin)
-    with jax.named_scope('o_on_2'):
-        output_on(2, begin)
-    with jax.named_scope('share_aside'):
-        share_aside(begin)
-    for d in range(3, Z):
-        with jax.named_scope('o_on_3'):
+        for a in range(HOLD):
+            for j in range(1, XH):
+                if act is begin:
+                    ja_side(a, j, from_tp(j)).wait_recv()
+                act(ja_twin(a, j, from_tp(j)))
+
+    share(0, begin)
+    for d in range(2, Z):
+        with jax.named_scope('o_on_2'):
             output_on(d, begin)
+        if d == 2:
+            with jax.named_scope('share'):
+                for k in range(1, Z):
+                    share(k, begin)
+            with jax.named_scope('share_aside'):
+                share_aside(begin)
     with jax.named_scope('share_wait'):
         for k in range(1, Z):
-            l_across(k, back_z(k)).wait_recv()
+            origin = back_z(k)
+            pl.when(is_holder(origin))(lambda: l_across(k, origin - offset).wait_recv())
         for k in range(XH):
             for zz in range(Z):
                 j_twin(zz, k, (twin + TP - 2 * k) % TP).wait_recv()
+            for a in range(HOLD):
+                ja_twin(a, k, (twin + TP - 2 * k) % TP).wait_recv()
 
     mem_base = TP * sinks.shape[0] * HD
     per_tp = sinks.shape[0] * HD
     half = N // 2
-    for zz in range(Z):
-        for t in range(TP):
-            at = t * per_tp + zz * LANES
-            X[:, at : at + LANES] = J[t, zz, :N, :]
+    pairs = CA // LANES - 1
+    for t in range(TP):
+        for a in range(HOLD):
+            for pair in range(pairs):
+                at = t * per_tp + (a * pairs + pair) * LANES
+                X[:, at : at + LANES] = JA[t, a, pair * N : (pair + 1) * N, :]
+        for zz in range(Z):
             at = mem_base + (t * Z + zz) * HD
-            X[:half, at : at + HD] = J[t, zz, N:, :HD]
-            X[half:, at : at + HD] = J[t, zz, N:, HD:]
-        totals[2 * zz : 2 * zz + 2, :] = LT[zz, 0:2, :]
-
-    with jax.named_scope('o_wait'):
-        keep[8].wait()
-        for zz in range(Z):
-            for k in range(1, Y):
-                for c in range(OC):
-                    o_side(zz, k, c, back_y(k), False).wait_recv()
-
-    tile = 256
-
-    def columns(i, nothing):
-        cols = pl.ds(pl.multiple_of(i * tile, tile), tile)
-        mixed[:, cols] = dot(X[...], O[:, cols]).astype(jnp.bfloat16)
+            X[:half, at : at + HD] = JM[t, zz, :, :HD]
+            X[half:, at : at + HD] = JM[t, zz, :, HD:]
+    for a in range(HOLD):
+        totals[2 * pairs * a : 2 * pairs * (a + 1), :] = LT[a, : 2 * pairs, :]
+
+    tile = min(256, M)
+    deep = Y * KO
+
+    def outputs(zz):
+        for k in range(1, Y):
+            for c in range(OC):
+                o_side(zz, k, c, back_y(k), False).wait_recv()
+        part = pl.ds(pl.multiple_of(zz * deep, deep), deep)
+
+        def columns(i, nothing):
+            cols = pl.ds(pl.multiple_of(i * tile, tile), tile)
+            MIX[:, cols] += dot(X[:, part], O[part, cols])
+            return nothing
+
+        lax.fori_loop(0, M // tile, columns, 0)
+
+    MIX[...] = jnp.zeros_like(MIX)
+    keep[7].wait()
+
+    def stage_three(d, nothing):
+        with jax.named_scope('outputs'):
+            both_sides(d, outputs)
         return nothing
 
-    with jax.named_scope('out_matmul'):
-        lax.fori_loop(0, mixed.shape[1] // tile, columns, 0)
+    lax.fori_loop(0, Z, stage_three, 0)
+    mixed[...] = MIX[...].astype(jnp.bfloat16)
 
     own_tokens(drain)
     weights_far(drain)
@@ -636,20 +805,23 @@
         f_across(k, z).wait_send()
 
     def settle(i, nothing):
-        near(i, drain)
         weights_on(i, drain)
         tokens_on(i, drain)
         output_on(i, drain)
         return nothing
 
+    for d in range(Z):
+        near(d, drain)
     lax.fori_loop(1, Z, settle, 0)
     for zz in range(Z):
         tokens_aside(zz, drain)
-        h_side(zz, (y + 1) // Y).wait_send()
+        pl.when(holds)(lambda: h_side(zz, (y + 1) // Y).wait_send())
         for k in range(1, Y):
             s_side(zz, k, y).wait_send()
-    hand_over(drain)
-    share(drain)
+    for k in range(1, Z):
+        hand_over(k, drain)
+    for k in range(Z):
+        share(k, drain)
     share_aside(drain)
 
 
@@ -660,13 +832,15 @@
     R, D = tokens.shape
     N = R * TP
     KD = weights[0].shape[0]
-    C = sum(part.shape[1] for part in weights[3:]) // Z + weights[0].shape[1] // Z + 2 * HD
-    TC = OC = 3
-    WC = 2
+    HOLD = weights[1].shape[1] // HD
+    CA = weights[0].shape[1] // HOLD + 2 * HD
+    CM = sum(part.shape[1] for part in weights[3:]) // Z
+    MC = 2
+    TC, OC = 3, 6
+    WC = 4
     M = w_out.shape[1]
     bf, f32 = jnp.bfloat16, jnp.float32
     dma = pltpu.SemaphoreType.DMA
-    piece = N + N // 2
     vmem = pl.BlockSpec(memory_space=pltpu.VMEM)
     smem = pl.BlockSpec(memory_space=pltpu.SMEM)
     hbm = pl.BlockSpec(memory_space=pl.ANY)
@@ -676,38 +850,47 @@
             jax.ShapeDtypeStruct((N, M), bf),
             jax.ShapeDtypeStruct((sinks.shape[0], N), f32),
         ],
-        in_specs=[vmem] * 3 + [hbm] * 9 + [smem] * 2,
-        out_specs=[vmem, vmem],
+        in_specs=[vmem] * 4 + [hbm] * 8 + [smem] * 2,
+        out_specs=[vmem] * 2,
         scratch_shapes=[pltpu.VMEM(part.shape, bf) for part in weights]
         + [
-            pltpu.VMEM((Z, KD, C), bf),
+            pltpu.VMEM((Z, KD, CM), bf),
+            pltpu.VMEM((HOLD, KD, CA), bf),
             pltpu.VMEM((Z * N, D), bf),
-            pltpu.VMEM((D, C), bf),
-            pltpu.VMEM(gates.shape, bf),
+            pltpu.VMEM((D, CM), bf),
+            pltpu.VMEM((D, CA), bf),
+            pltpu.VMEM((D, LANES), bf),
             pltpu.VMEM((S * w_out.shape[0], M), bf),
-            pltpu.VMEM((Z * N, C + LANES), f32),
+            pltpu.VMEM((Z * N, CM + LANES), f32),
+            pltpu.VMEM((Z * N, CA), f32),
             pltpu.VMEM((LANES, N), f32),
-            pltpu.VMEM((Z * N, C), bf),
+            pltpu.VMEM((Z * N, CM), bf),
+            pltpu.VMEM((Z * N, CA), bf),
             pltpu.VMEM((Z * N, LANES), f32),
             pltpu.VMEM((S, HD, LANES), f32),
             pltpu.VMEM((Z, HD, LANES), f32),
             pltpu.VMEM((Z + 1, WINDOW, LANES), bf),
             pltpu.VMEM((Z, 8, N), f32),
             pltpu.VMEM((Z, 8, N), f32),
-            pltpu.VMEM((Z, piece, LANES), bf),
-            pltpu.VMEM((TP, Z, piece, LANES), bf),
+            pltpu.VMEM((Z, N // 2, LANES), bf),
+            pltpu.VMEM((Z, N * (CA // LANES - 1), LANES), bf),
+            pltpu.VMEM((TP, Z, N // 2, LANES), bf),
+            pltpu.VMEM((TP, HOLD, N * (CA // LANES - 1), LANES), bf),
             pltpu.VMEM((Z, 8, N), f32),
-            pltpu.VMEM((Z, 8, N), f32),
+            pltpu.VMEM((HOLD, 8, N), f32),
             pltpu.VMEM((N, S * w_out.shape[0]), bf),
-            dma((9,)),
-            dma((2, Z, WC)), dma((2, Z, WC)), dma((Y - 1, Z, WC)), dma((Y - 1, Z, WC)),
+            pltpu.VMEM((N, M), f32),
+            dma((8,)),
+            dma((2, Z, MC)), dma((2, Z, MC)), dma((2, Z, WC)), dma((2, Z, WC)),
+            dma((Y - 1, Z, MC)), dma((Y - 1, Z, MC)), dma((Y - 1, Z, WC)), dma((Y - 1, Z, WC)),
             dma((Z,)), dma((Z,)),
             dma((2, Z, TC)), dma((Z, TC)), dma((XH - 1, Z, TC)), dma((XH - 1, Z, TC)),
             dma((XH, Z, TC)), dma((XH, Z, TC)),
             dma((2, Z, OC)), dma((Z, OC)), dma((Y - 1, Z, OC)), dma((Y - 1, Z, OC)),
             dma((Z,)), dma((Z,)), dma((Y - 1, Z)), dma((Y - 1, Z)),
-            dma((Z,)), dma((Z,)), dma((Z,)), dma((Z,)),
+            dma((Z,)), dma((Z,)), dma((Z,)), dma((Z,)), dma((Z,)), dma((Z,)),
             dma((XH - 1, Z)), dma((XH - 1, Z)), dma((XH, Z)), dma((XH, Z)),
+            dma((XH - 1, HOLD)), dma((XH - 1, HOLD)), dma((XH, HOLD)), dma((XH, HOLD)),
         ],
         compiler_params=pltpu.CompilerParams(
             collective_id=0, has_side_effects=True, vmem_limit_bytes=60 * 2**20
@@ -736,7 +919,7 @@
         tokens,
         norm_gain[None, :],
         forget_shift.T,
-        w_gates.reshape(w_gates.shape[0], -1),
+        w_gates.transpose(1, 2, 0).reshape(-1, w_gates.shape[0]),
         w_out,
         weights,
         sinks,

time: 197 us -> 171 us (0.87)
  Pallas kernels: 191 us -> 168 us
  local copies, waits for them, and re-layouts: 4.94 us -> 2.67 us
    pallas_call x1, Pallas kernels: 191 us -> 168 us  [mix(): pl.pallas_call(functools.partial(mixer_kernel, (Z, Y, TP, TC, WC, OC)), o...]
    reshape x1 -> x0, local copies, waits for them, and re-layouts: 2.27 us -> none  [shards(): w_gates.reshape(w_gates.shape[0], -1)]
where the time goes in v2:
time: 171 us
  Pallas kernels  168 us (98%)
  local copies, waits for them, and re-layouts  2.67 us (2%)
    pallas_call x1, Pallas kernels, mix(): pl.pallas_call(functools.partial(mixer_kernel, (Z, Y, TP, TC, WC, OC)), o...  168 us

profile of v2, /device:TPU:0, one launch (start us, length us, event | category | flops | bytes accessed | tf_op | source)
XLA Modules:
  0.0 171.2 jit_solution(1502726258998004997)
XLA Ops:
  0.6 167.8 %shard_map.149 = (bf16[384,1024]{1,0:T(8,128)(2,1)}, f32[8,384]{1,0:T(8,128)}) custom-call(bf16[96,4096]{1,0:T(8,128)(2,1)} %tokens.1, f32[1,4096]{1,0:T(1,128)} %bitcast.7, f32[4,384]{1,0:T(4,128)} %bitcast.9, bf16[32,4096]{1,0:T(8,128)(2,1)} %bitcast.6, bf16[384,1024]{1,0:T(8,128)(2,1)} %w_out.1, bf16[512,512]{1,0:T(8,128)(2,1)} %w_query.1, ...), custom_call_target="tpu_custom_call" | custom-call | tf_op jit(solution)/shard_map/pallas_call | solution.py:847
  168.5 0.0 copy-start
  168.5 2.1 %copy.18 = bf16[384,1024]{1,0:T(8,128)(2,1)} copy(bf16[384,1024]{1,0:T(8,128)(2,1)} %get-tuple-element.8) | data formatting | bytes 1572864
  170.6 0.0 copy-done
  170.6 0.6 copy.19
Async XLA Ops:
  168.5 2.1 %copy-start = (f32[8,384]{1,0:T(8,128)S(1)}, f32[8,384]{1,0:T(8,128)}, u32[]{:S(2)}) copy-start(f32[8,384]{1,0:T(8,128)} %get-tuple-element.5) | copy-start | bytes 36868

commit v3 on v2

--- a/solution.py
+++ b/solution.py
@@ -22,6 +22,10 @@
 
 def drain(copy):
     copy.wait_send()
+
+
+def each(count, act):
+    return range(count) if act is begin else (None,)
 
 
 def dot(left, right, **more):
@@ -73,6 +77,14 @@
             device_id={"sp": to_sp, "tp": to_tp}, device_id_type=MESH,
         )
 
+    def span(base, c, count, size):
+        if c is None:
+            return pl.ds(pl.multiple_of(base, size), count * size)
+        return pl.ds(pl.multiple_of(base + c * size, size), size)
+
+    def slot(c):
+        return 0 if c is None else c
+
     def side_tp(k):
         return (tp + 2 * k) % TP
 
@@ -92,35 +104,35 @@
         return (y + Y - k) % Y
 
     def m_rows(zz, yy, c):
-        return WM.at[pl.ds(pl.multiple_of((zz * Y + yy) * KD + c * RM, RM), RM), :]
+        return WM.at[span((zz * Y + yy) * KD, c, MC, RM), :]
 
     def a_rows(zz, yy, c):
-        return WA.at[pl.ds(pl.multiple_of((zz * Y + yy) * KD + c * RW, RW), RW), :]
+        return WA.at[span((zz * Y + yy) * KD, c, WC, RW), :]
 
     def m_across(way, d, c, source, piece):
         to = z + d * (1 - 2 * way)
         return remote(
-            PM.at[piece, pl.ds(c * RM, RM), :], m_rows(source, y, c),
-            w_send.at[way, d, c], w_recv.at[way, d, c], to * Y + y, tp,
+            PM.at[piece, span(0, c, MC, RM), :], m_rows(source, y, c),
+            w_send.at[to], w_recv.at[source, slot(c)], to * Y + y, tp,
         )
 
     def a_across(way, d, c, source, piece):
         to = z + d * (1 - 2 * way)
         return remote(
-            PA.at[piece, pl.ds(c * RW, RW), :], a_rows(source, y, c),
-            wa_send.at[way, d, c], wa_recv.at[way, d, c], to * Y + y, tp,
+            PA.at[piece, span(0, c, WC, RW), :], a_rows(source, y, c),
+            wa_send.at[to], wa_recv.at[source, slot(c)], to * Y + y, tp,
         )
 
     def m_side(zz, j, c, source):
         place = m_rows(zz, source, c)
         return remote(
-            place, place, wy_send.at[j - 1, zz, c], wy_recv.at[j - 1, zz, c], z * Y + up_y(j), tp
+            place, place, wy_send.at[j - 1, zz], wy_recv.at[j - 1, zz, slot(c)], z * Y + up_y(j), tp
         )
 
     def a_side(zz, j, c, source):
         place = a_rows(zz, source, c)
         return remote(
-            place, place, wb_send.at[j - 1, zz, c], wb_recv.at[j - 1, zz, c], z * Y + up_y(j), tp
+            place, place, wb_send.at[j - 1, zz], wb_recv.at[j - 1, zz, slot(c)], z * Y + up_y(j), tp
         )
 
     def f_across(k, source):
@@ -129,36 +141,34 @@
         )
 
     def t_rows(zz, tt, c):
-        start = pl.multiple_of((zz * TP + tt) * R + c * RC, RC)
-        return T.at[pl.ds(start, RC), :]
+        return T.at[span((zz * TP + tt) * R, c, TC, RC), :]
 
     def t_line(zz, way, c):
         place = t_rows(zz, tp, c)
         to = (z + 1 - 2 * way) * Y + y
-        return remote(place, place, tz_send.at[way, zz, c], tz_recv.at[zz, c], to, tp)
+        return remote(place, place, tz_send.at[way, zz], tz_recv.at[zz, slot(c)], to, tp)
 
     def t_side(zz, k, c, source):
         place = t_rows(zz, source, c)
-        return remote(place, place, tx_send.at[k - 1, zz, c], tx_recv.at[k - 1, zz, c], sp, side_tp(k))
+        return remote(place, place, tx_send.at[k - 1, zz], tx_recv.at[k - 1, zz, slot(c)], sp, side_tp(k))
 
     def t_twin(zz, k, c, source):
         place = t_rows(zz, source, c)
-        return remote(place, place, tt_send.at[k, zz, c], tt_recv.at[k, zz, c], sp, twin)
+        return remote(place, place, tt_send.at[k, zz], tt_recv.at[k, zz, slot(c)], sp, twin)
 
     def o_rows(zz, yy, c):
-        start = pl.multiple_of((zz * Y + yy) * KO + c * RO, RO)
-        return O.at[pl.ds(start, RO), :]
+        return O.at[span((zz * Y + yy) * KO, c, OC, RO), :]
 
     def o_line(zz, way, c, own):
         place = o_rows(zz, y, c)
-        src = w_out.at[pl.ds(c * RO, RO), :] if own else place
+        src = w_out.at[span(0, c, OC, RO), :] if own else place
         to = (z + 1 - 2 * way) * Y + y
-        return remote(src, place, oz_send.at[way, zz, c], oz_recv.at[zz, c], to, tp)
+        return remote(src, place, oz_send.at[way, zz], oz_recv.at[zz, slot(c)], to, tp)
 
     def o_side(zz, k, c, source, own):
         place = o_rows(zz, source, c)
-        src = w_out.at[pl.ds(c * RO, RO), :] if own else place
-        return remote(src, place, oy_send.at[k - 1, zz, c], oy_recv.at[k - 1, zz, c], z * Y + up_y(k), tp)
+        src = w_out.at[span(0, c, OC, RO), :] if own else place
+        return remote(src, place, oy_send.at[k - 1, zz], oy_recv.at[k - 1, zz, slot(c)], z * Y + up_y(k), tp)
 
     def h_side(zz, shift):
         rows = pl.ds(pl.multiple_of(zz * N + N - WINDOW, WINDOW), WINDOW)
@@ -277,10 +287,10 @@
 
         @pl.when(is_holder(to))
         def _():
-            for c in range(WC):
+            for c in each(WC, act):
                 act(a_across(way, d, c, z, to - offset))
 
-        for c in range(MC):
+        for c in each(MC, act):
             act(m_across(way, d, c, z, to))
 
     def weights_far(act):
@@ -290,12 +300,12 @@
 
     def weights_aside(zz, act):
         for j in range(1, Y):
-            for c in range(MC):
+            for c in each(MC, act):
                 act(m_side(zz, j, c, y))
 
             @pl.when(holds)
             def _():
-                for c in range(WC):
+                for c in each(WC, act):
                     act(a_side(zz, j, c, y))
 
     def weights_on(d, act):
@@ -303,14 +313,14 @@
             origin = z - d * (1 - 2 * way)
 
             def landed_a(way=way, origin=origin):
-                for c in range(WC):
+                for c in each(WC, act):
                     if act is begin:
                         a_across(way, d, c, origin, 0).wait_recv()
                     for j in range(1, Y):
                         act(a_side(origin, j, c, y))
 
             def landed_m(way=way, origin=origin):
-                for c in range(MC):
+                for c in each(MC, act):
                     if act is begin:
                         m_across(way, d, c, origin, 0).wait_recv()
                     for j in range(1, Y):
@@ -320,19 +330,19 @@
             pl.when(there)(landed_m)
 
     def own_tokens(act):
-        for c in range(TC):
+        for c in each(TC, act):
             pl.when(can_up)(lambda: act(t_line(z, 0, c)))
             pl.when(can_down)(lambda: act(t_line(z, 1, c)))
             for k in range(1, XH):
                 act(t_side(z, k, c, tp))
             act(t_twin(z, 0, c, tp))
 
-    def tokens_on(d, act):
+    def tokens_on(d, act, some=None):
         for way, origin, there, further in (
             (0, z - d, z - d >= 0, can_up), (1, z + d, z + d < Z, can_down),
         ):
             def landed(way=way, origin=origin, further=further):
-                for c in range(TC):
+                for c in each(TC, act) if some is None else some:
                     if act is begin:
                         t_line(origin, way, c).wait_recv()
                     pl.when(further)(lambda: act(t_line(origin, way, c)))
@@ -344,18 +354,18 @@
 
     def tokens_aside(zz, act):
         for k in range(1, XH):
-            for c in range(TC):
+            for c in each(TC, act):
                 if act is begin:
                     t_side(zz, k, c, from_tp(k)).wait_recv()
                 act(t_twin(zz, k, c, from_tp(k)))
 
     def output_aside(act):
-        for c in range(OC):
+        for c in each(OC, act):
             for k in range(1, Y):
                 act(o_side(z, k, c, y, True))
 
     def own_output(act):
-        for c in range(OC):
+        for c in each(OC, act):
             pl.when(can_up)(lambda: act(o_line(z, 0, c, True)))
             pl.when(can_down)(lambda: act(o_line(z, 1, c, True)))
 
@@ -364,7 +374,7 @@
             (0, z - d, z - d >= 0, can_up), (1, z + d, z + d < Z, can_down),
         ):
             def landed(way=way, origin=origin, further=further):
-                for c in range(OC):
+                for c in each(OC, act):
                     if act is begin and line:
                         o_line(origin, way, c, False).wait_recv()
                     if line:
@@ -389,19 +399,21 @@
 
     depth = Y * KD
 
-    def project(zk):
+    def project(zk, b):
         cols = pl.ds(pl.multiple_of(zk * depth, depth), depth)
 
+        rows = block_rows(b)
+        block = T[rows, cols]
+        ACC[rows, :CM] += dot(block, WM[cols, :])
+        ACC[rows, CM:] += dot(block, GW[cols, :])
+
+        @pl.when(holds)
+        def _():
+            ACCA[rows, :] += dot(block, WA[cols, :])
+
+    def project_all(zk):
         def part(b, nothing):
-            rows = block_rows(b)
-            block = T[rows, cols]
-            ACC[rows, :CM] += dot(block, WM[cols, :])
-            ACC[rows, CM:] += dot(block, GW[cols, :])
-
-            @pl.when(holds)
-            def _():
-                ACCA[rows, :] += dot(block, WA[cols, :])
-
+            project(zk, b)
             return nothing
 
         lax.fori_loop(0, Z, part, 0)
@@ -554,27 +566,50 @@
 
         lax.fori_loop(0, 2, one, 0)
 
+    def arrived(zz):
+        for k in range(XH):
+            for c in range(TC):
+                t_twin(zz, k, c, (twin + TP - 2 * k) % TP).wait_recv()
+
+    def weights_here(zz):
+        for j in range(1, Y):
+            for c in range(MC):
+                m_side(zz, j, c, back_y(j)).wait_recv()
+
+            @pl.when(holds)
+            def _():
+                for c in range(WC):
+                    a_side(zz, j, c, back_y(j)).wait_recv()
+
+    def early(zz):
+        arrived(zz)
+        project(z, zz)
+
     def stage(d, nothing):
         with jax.named_scope('t_on'):
-            tokens_on(d, begin)
+            pl.when(d < Z - 1)(lambda: tokens_on(d, begin))
+            pl.when(d == Z - 1)(lambda: tokens_on(d, begin, range(TC)))
         near(d, begin)
-
         inside = can_up & can_down
 
-        @pl.when((d == Z - 1) & jnp.logical_not(inside))
+        @pl.when(d == Z - 1)
         def _():
             weights_far(begin)
-
-        @pl.when((d == Z - 1) & inside)
-        def _():
-            weights_far(begin)
-
-        pl.when(d == Z - 1)(lambda: own_output(begin))
+            own_output(begin)
+            with jax.named_scope('t_on_rest'):
+                tokens_on(d, begin, range(TC, TC))
 
         @pl.when((d == 2) & inside)
         def _():
             with jax.named_scope('w_on_mid'):
                 weights_on(1, begin)
+
+        @pl.when(d == Z - 1)
+        def _():
+            with jax.named_scope('early'):
+                weights_here(z)
+                for near_d in range(Z - 2):
+                    both_sides(near_d, early)
 
         with jax.named_scope('t_aside'):
             both_sides(d - 1, lambda zz: tokens_aside(zz, begin))
@@ -586,26 +621,20 @@
             weights_on(d, begin)
     with jax.named_scope('t_last'):
         both_sides(Z - 1, lambda zz: tokens_aside(zz, begin))
-        for zz in range(Z):
-            for k in range(XH):
-                for c in range(TC):
-                    t_twin(zz, k, c, (twin + TP - 2 * k) % TP).wait_recv()
+        for d in range(max(Z - 2, 0), Z):
+            both_sides(d, arrived)
 
     def multiply(zz):
         with jax.named_scope('w_side'):
-            for j in range(1, Y):
-                for c in range(MC):
-                    m_side(zz, j, c, back_y(j)).wait_recv()
-
-                @pl.when(holds)
-                def _():
-                    for c in range(WC):
-                        a_side(zz, j, c, back_y(j)).wait_recv()
-
+            weights_here(zz)
         with jax.named_scope('project'):
-            project(zz)
-
-    both_sides(0, multiply)
+            project_all(zz)
+
+    def late(zz):
+        project(z, zz)
+
+    for d in range(max(Z - 2, 0), Z):
+        both_sides(d, late)
 
     @pl.when(jnp.logical_not(can_up & can_down))
     def _():
@@ -627,13 +656,13 @@
 
     def local(zz, nothing):
         local_work(zz)
-        for i in range(4):
-            pl.when(zz == i)(lambda: output_pieces(i, 1 + i, begin))
+        for i in range(2):
+            pl.when(zz == Z - 3 + 2 * i)(lambda: output_pieces(i, 1 + i, begin))
         return nothing
 
     lax.fori_loop(0, Z, local, 0)
 
-    output_pieces(4, 2 * OC, begin)
+    output_pieces(2, 2 * OC, begin)
 
     with jax.named_scope('halo_state'):
         for zz in range(Z):
@@ -734,6 +763,36 @@
                 act(ja_twin(a, j, from_tp(j)))
 
     share(0, begin)
+
+    def settle():
+        own_tokens(drain)
+        weights_far(drain)
+        weights_aside(z, drain)
+        for k in range(1, Z):
+            f_across(k, z).wait_send()
+        for d in range(Z):
+            near(d, drain)
+
+        def one(i, nothing):
+            weights_on(i, drain)
+            tokens_on(i, drain)
+            return nothing
+
+        lax.fori_loop(1, Z, one, 0)
+
+        def two(zz, nothing):
+            tokens_aside(zz, drain)
+            pl.when(holds)(lambda: h_side(zz, (y + 1) // Y).wait_send())
+            for k in range(1, Y):
+                s_side(zz, k, y).wait_send()
+            return nothing
+
+        lax.fori_loop(0, Z, two, 0)
+        output_aside(drain)
+        own_output(drain)
+
+    with jax.named_scope('settle'):
+        settle()
     for d in range(2, Z):
         with jax.named_scope('o_on_2'):
             output_on(d, begin)
@@ -786,6 +845,13 @@
         lax.fori_loop(0, M // tile, columns, 0)
 
     MIX[...] = jnp.zeros_like(MIX)
+    with jax.named_scope('settle_j'):
+        output_on(1, drain)
+        for k in range(1, Z):
+            hand_over(k, drain)
+        for k in range(Z):
+            share(k, drain)
+        share_aside(drain)
     keep[7].wait()
 
     def stage_three(d, nothing):
@@ -794,35 +860,12 @@
         return nothing
 
     lax.fori_loop(0, Z, stage_three, 0)
-    mixed[...] = MIX[...].astype(jnp.bfloat16)
-
-    own_tokens(drain)
-    weights_far(drain)
-    weights_aside(z, drain)
-    output_aside(drain)
-    own_output(drain)
-    for k in range(1, Z):
-        f_across(k, z).wait_send()
-
-    def settle(i, nothing):
-        weights_on(i, drain)
-        tokens_on(i, drain)
-        output_on(i, drain)
-        return nothing
-
-    for d in range(Z):
-        near(d, drain)
-    lax.fori_loop(1, Z, settle, 0)
-    for zz in range(Z):
-        tokens_aside(zz, drain)
-        pl.when(holds)(lambda: h_side(zz, (y + 1) // Y).wait_send())
-        for k in range(1, Y):
-            s_side(zz, k, y).wait_send()
-    for k in range(1, Z):
-        hand_over(k, drain)
-    for k in range(Z):
-        share(k, drain)
-    share_aside(drain)
+    with jax.named_scope('cast'):
+        mixed[...] = MIX[...].astype(jnp.bfloat16)
+
+    with jax.named_scope('drain'):
+        for d in range(2, Z):
+            output_on(d, drain)
 
 
 def mix(tokens, gain, shifts, gates, w_out, weights, sinks, bias):
@@ -836,7 +879,7 @@
     CA = weights[0].shape[1] // HOLD + 2 * HD
     CM = sum(part.shape[1] for part in weights[3:]) // Z
     MC = 2
-    TC, OC = 3, 6
+    TC = OC = 3
     WC = 4
     M = w_out.shape[1]
     bf, f32 = jnp.bfloat16, jnp.float32
@@ -881,12 +924,12 @@
             pltpu.VMEM((N, S * w_out.shape[0]), bf),
             pltpu.VMEM((N, M), f32),
             dma((8,)),
-            dma((2, Z, MC)), dma((2, Z, MC)), dma((2, Z, WC)), dma((2, Z, WC)),
-            dma((Y - 1, Z, MC)), dma((Y - 1, Z, MC)), dma((Y - 1, Z, WC)), dma((Y - 1, Z, WC)),
+            dma((Z,)), dma((Z, MC)), dma((Z,)), dma((Z, WC)),
+            dma((Y - 1, Z)), dma((Y - 1, Z, MC)), dma((Y - 1, Z)), dma((Y - 1, Z, WC)),
             dma((Z,)), dma((Z,)),
-            dma((2, Z, TC)), dma((Z, TC)), dma((XH - 1, Z, TC)), dma((XH - 1, Z, TC)),
-            dma((XH, Z, TC)), dma((XH, Z, TC)),
-            dma((2, Z, OC)), dma((Z, OC)), dma((Y - 1, Z, OC)), dma((Y - 1, Z, OC)),
+            dma((2, Z)), dma((Z, TC)), dma((XH - 1, Z)), dma((XH - 1, Z, TC)),
+            dma((XH, Z)), dma((XH, Z, TC)),
+            dma((2, Z)), dma((Z, OC)), dma((Y - 1, Z)), dma((Y - 1, Z, OC)),
             dma((Z,)), dma((Z,)), dma((Y - 1, Z)), dma((Y - 1, Z)),
             dma((Z,)), dma((Z,)), dma((Z,)), dma((Z,)), dma((Z,)), dma((Z,)),
             dma((XH - 1, Z)), dma((XH - 1, Z)), dma((XH, Z)), dma((XH, Z)),

time: 171 us -> 168 us (0.982)
  Pallas kernels: 168 us -> 164 us
    pallas_call x1, Pallas kernels: 168 us -> 164 us  [mix(): pl.pallas_call(functools.partial(mixer_kernel, (Z, Y, TP, TC, WC, OC)), o...]
where the time goes in v3:
time: 168 us; the launch traced here: 167 us
  Pallas kernels  164 us (98%)
  local copies, waits for them, and re-layouts  2.67 us (2%)
    pallas_call x1, Pallas kernels, mix(): pl.pallas_call(functools.partial(mixer_kernel, (Z, Y, TP, TC, WC, OC)), o...  164 us

profile of v3, /device:TPU:0, one launch (start us, length us, event | category | flops | bytes accessed | tf_op | source)
XLA Modules:
  0.0 167.2 jit_solution(17769602625581151075)
XLA Ops:
  0.6 163.8 %shard_map.149 = (bf16[384,1024]{1,0:T(8,128)(2,1)}, f32[8,384]{1,0:T(8,128)}) custom-call(bf16[96,4096]{1,0:T(8,128)(2,1)} %tokens.1, f32[1,4096]{1,0:T(1,128)} %bitcast.7, f32[4,384]{1,0:T(4,128)} %bitcast.9, bf16[32,4096]{1,0:T(8,128)(2,1)} %bitcast.6, bf16[384,1024]{1,0:T(8,128)(2,1)} %w_out.1, bf16[512,512]{1,0:T(8,128)(2,1)} %w_query.1, ...), custom_call_target="tpu_custom_call" | custom-call | tf_op jit(solution)/shard_map/pallas_call | solution.py:890
  164.5 0.0 copy-start
  164.5 2.1 %copy.18 = bf16[384,1024]{1,0:T(8,128)(2,1)} copy(bf16[384,1024]{1,0:T(8,128)(2,1)} %get-tuple-element.8) | data formatting | bytes 1572864
  166.6 0.0 copy-done
  166.6 0.6 copy.19
Async XLA Ops:
  164.5 2.1 %copy-start = (f32[8,384]{1,0:T(8,128)S(1)}, f32[8,384]{1,0:T(8,128)}, u32[]{:S(2)}) copy-start(f32[8,384]{1,0:T(8,128)} %get-tuple-element.5) | copy-start | bytes 36868

commit v4 on v3

--- a/solution.py
+++ b/solution.py
@@ -653,11 +653,12 @@
 
     with jax.named_scope('o_line_1'):
         output_on(1, begin, aside=False)
+        output_pieces(0, 1, begin)
 
     def local(zz, nothing):
         local_work(zz)
-        for i in range(2):
-            pl.when(zz == Z - 3 + 2 * i)(lambda: output_pieces(i, 1 + i, begin))
+        for i in range(1):
+            pl.when(zz == Z - 1 + i)(lambda: output_pieces(1 + i, 1 + 1 + i, begin))
         return nothing
 
     lax.fori_loop(0, Z, local, 0)

time: 168 us -> 165 us (0.982)
  Pallas kernels: 164 us -> 161 us
    pallas_call x1, Pallas kernels: 164 us -> 161 us  [mix(): pl.pallas_call(functools.partial(mixer_kernel, (Z, Y, TP, TC, WC, OC)), o...]
where the time goes in v4:
time: 165 us; the launch traced here: 164 us
  Pallas kernels  161 us (98%)
  local copies, waits for them, and re-layouts  2.67 us (2%)
    pallas_call x1, Pallas kernels, mix(): pl.pallas_call(functools.partial(mixer_kernel, (Z, Y, TP, TC, WC, OC)), o...  161 us

profile of v4, /device:TPU:0, one launch (start us, length us, event | category | flops | bytes accessed | tf_op | source)
XLA Modules:
  0.0 163.9 jit_solution(7965198006287920351)
XLA Ops:
  0.6 160.6 %shard_map.149 = (bf16[384,1024]{1,0:T(8,128)(2,1)}, f32[8,384]{1,0:T(8,128)}) custom-call(bf16[96,4096]{1,0:T(8,128)(2,1)} %tokens.1, f32[1,4096]{1,0:T(1,128)} %bitcast.7, f32[4,384]{1,0:T(4,128)} %bitcast.9, bf16[32,4096]{1,0:T(8,128)(2,1)} %bitcast.6, bf16[384,1024]{1,0:T(8,128)(2,1)} %w_out.1, bf16[512,512]{1,0:T(8,128)(2,1)} %w_query.1, ...), custom_call_target="tpu_custom_call" | custom-call | tf_op jit(solution)/shard_map/pallas_call | solution.py:891
  161.2 0.0 copy-start
  161.3 2.1 %copy.18 = bf16[384,1024]{1,0:T(8,128)(2,1)} copy(bf16[384,1024]{1,0:T(8,128)(2,1)} %get-tuple-element.8) | data formatting | bytes 1572864
  163.3 0.0 copy-done
  163.3 0.6 copy.19
Async XLA Ops:
  161.2 2.1 %copy-start = (f32[8,384]{1,0:T(8,128)S(1)}, f32[8,384]{1,0:T(8,128)}, u32[]{:S(2)}) copy-start(f32[8,384]{1,0:T(8,128)} %get-tuple-element.5) | copy-start | bytes 36868
